TPU v7x, 32 devices: a whole 2x2x4 slice. The times are simulated.
32 devices in a mesh: sp: 4 (over z), tp: 8 (over y, x, core).
Axes of the slice: x: 2, y: 2, z: 4, core: 2. Of those that a mesh axis runs over, the one named last changes fastest.
Arguments:
- latent: bfloat16 [1024, 4096], P(('sp', 'tp')), may hold values from -16 to 16
- context: bfloat16 [256, 4096], P('sp'), may hold values from -16 to 16
- cond: bfloat16 [4096], P('sp'), may hold values from -6 to 6
- cond_ctx: bfloat16 [4096], P('sp'), may hold values from -6 to 6
- mod_shift_w: bfloat16 [4096, 4096], P('sp', 'tp'), may hold values from -0.15625 to 0.15625
- mod_scale_w: bfloat16 [4096, 4096], P('sp', 'tp'), may hold values from -0.15625 to 0.15625
- mod_gate_w: bfloat16 [4096, 4096], P('sp', 'tp'), may hold values from -0.15625 to 0.15625
- norm_gain: bfloat16 [4096], replicated, may hold values from 0.099609375 to 1.8984375
- proj_z: bfloat16 [4096, 4096], P(None, 'tp'), may hold values from -0.09375 to 0.09375
- proj_x: bfloat16 [4096, 4096], P(None, 'tp'), may hold values from -0.09375 to 0.09375
- proj_b: bfloat16 [4096, 8192], P(None, 'tp'), may hold values from -0.09375 to 0.09375
- proj_c: bfloat16 [4096, 8192], P(None, 'tp'), may hold values from -0.09375 to 0.09375
- proj_dt: bfloat16 [4096, 128], replicated, may hold values from -0.09375 to 0.09375
- conv_x: bfloat16 [3, 4096], P(None, 'tp'), may hold values from -3.5 to 3.5
- conv_b: bfloat16 [3, 8192], P(None, 'tp'), may hold values from -3.5 to 3.5
- conv_c: bfloat16 [3, 8192], P(None, 'tp'), may hold values from -3.5 to 3.5
- dt_bias: float32 [128], P('tp'), may hold values from -1 to 1
- decay_log: float32 [128], P('tp'), may hold values from -11.6 to -2.9
- head_gain: bfloat16 [4096], P('tp'), may hold values from 0.099609375 to 1.8984375
- proj_out: bfloat16 [4096, 4096], P(None, 'tp'), may hold values from -0.09375 to 0.09375
Outputs:
- mixed: bfloat16 [1024, 4096], P(('sp', 'tp'))
All inputs are finite; a program needn't handle non-finite values.
Results may differ from a plain program's by a relative error of at most 0.0065.
Values may be sent and summed in bfloat16 or wider, within the bound.
No kernel may reach another device: no remote copies, remote signals or barrier semaphores. Data moves between devices by JAX's collectives and lax.ppermute only.
A program may use at most 128 MiB of HBM per device.

v0:
```python
import functools

import jax
import jax.numpy as jnp
from jax import lax
from jax.experimental import pallas as pl
from jax.experimental.pallas import tpu as pltpu
from jax.sharding import PartitionSpec as P


HEAD_DIM = 64
LANES = 128
EPS = 1e-06
F32 = jnp.float32
BF16 = jnp.bfloat16
VMEM = pl.BlockSpec(memory_space=pltpu.VMEM)
HBM = pl.BlockSpec(memory_space=pltpu.HBM)
MIB = 1024 * 1024
MOST = 63
HINT, HINT_BYTES = 2 * 10**10, 10**8


def silu(u):
    return u * (0.5 * jnp.tanh(0.5 * u) + 0.5)


def size_of(shape):
    count = 1
    for extent in shape.shape:
        count *= extent
    return count * jnp.dtype(shape.dtype).itemsize


def call(kernel, outs, inputs, specs, scratch=(), flops=0, moved=0, spare=4):
    held = sum(min(size_of(x), MIB) for x in inputs)
    held += sum(size_of(x) for x in jax.tree.leaves(outs))
    held += sum(size_of(x) for x in scratch if hasattr(x, "shape") and x.memory_space == pltpu.VMEM)
    return pl.pallas_call(
        kernel,
        out_shape=outs,
        in_specs=specs,
        out_specs=jax.tree.map(lambda _: VMEM, outs),
        scratch_shapes=list(scratch),
        compiler_params=pltpu.CompilerParams(vmem_limit_bytes=min(MOST * MIB, held + spare * MIB)),
        cost_estimate=pl.CostEstimate(flops=flops, bytes_accessed=moved, transcendentals=0),
    )(*inputs)


def shift(array, axis, step):
    count = lax.axis_size(axis)
    return lax.ppermute(array, axis, [(i, (i + step) % count) for i in range(count)])


def swap(array, bits):
    count = lax.axis_size("tp")
    return lax.ppermute(array, "tp", [(i, i ^ bits) for i in range(count)])


def direct(tp_count):
    return tp_count <= 8 and tp_count & (tp_count - 1) == 0 and tp_count > 1


def exchange_tp(array, dim, relay=True):
    count = lax.axis_size("tp")
    if not direct(count):
        return [lax.all_gather(array, "tp", axis=dim, tiled=True)]
    pieces = [array] + [None] * (count - 1)
    for q in range(2, count, 2):
        pieces[q] = swap(array, q)
    for q in range(0, count, 2):
        if relay:
            pieces[q + 1] = swap(pieces[q], 1)
        else:
            pieces[q + 1] = swap(array, q + 1)
    return pieces


def lane_rows(vector):
    return vector.reshape(-1, LANES) if vector.shape[0] % LANES == 0 else vector[None]


def one_row(rows):
    return jnp.concatenate([rows[i : i + 1, :] for i in range(rows.shape[0])], axis=1)


def mod_kernel(cond, cond_ctx, rows, w_shift, w_scale, w_gate, up, down):
    width = w_shift.shape[1]
    acts = [silu(one_row(c[...].astype(F32))) for c in (cond, cond_ctx)]
    both = jnp.concatenate(acts, axis=0).astype(BF16)
    parts = [jnp.dot(both, w[...], preferred_element_type=F32) for w in (w_shift, w_scale, w_gate)]
    mods = jnp.concatenate(parts + [jnp.zeros((2, width), F32)], axis=0)
    pieces = rows.shape[1] // width
    first = rows[0:1, :].astype(F32)
    last = rows[rows.shape[0] - 1 :, :].astype(F32)
    for out, row in ((up, last), (down, first)):
        out[0:8, :] = mods
        for r in range(pieces):
            out[8 + r : 9 + r, :] = row[:, r * width : (r + 1) * width]


def mod_parts(cond, cond_ctx, latent, w_shift, w_scale, w_gate):
    width = w_shift.shape[1]
    shape = jax.ShapeDtypeStruct((8 + latent.shape[1] // width, width), F32)
    return call(
        mod_kernel,
        [shape, shape],
        [lane_rows(cond), lane_rows(cond_ctx), latent, w_shift, w_scale, w_gate],
        [VMEM] * 6,
        flops=12 * w_shift.size,
        moved=6 * w_shift.size,
        spare=MOST,
    )


def assemble_kernel(*refs):
    pieces, mods, halo = refs[:-2], refs[-2], refs[-1]
    tp = lax.axis_index("tp")
    count = len(pieces)
    width = pieces[0].shape[1]
    halo[...] = jnp.zeros_like(halo)
    for q, piece in enumerate(pieces):
        source = tp ^ q
        mods[:, pl.ds(pl.multiple_of(source * width, width), width)] = piece[0:8, :]
        for at, owner in ((0, count - 1), (1, 0)):

            @pl.when(source == owner)
            def _(at=at, piece=piece):
                for r in range(count):
                    halo[at : at + 1, r * width : (r + 1) * width] = piece[8 + r : 9 + r, :]


def assemble(pieces, tp_count):
    if direct(tp_count):
        width = pieces[0].shape[1] * tp_count
        return call(
            assemble_kernel,
            [jax.ShapeDtypeStruct((8, width), F32), jax.ShapeDtypeStruct((8, width), F32)],
            pieces,
            [VMEM] * len(pieces),
            flops=HINT,
            moved=HINT_BYTES,
        )
    (whole,) = pieces
    width = whole.shape[1]
    part = width // tp_count
    before = whole[8:, width - part :].reshape(1, width)
    after = whole[8:, :part].reshape(1, width)
    return whole[:8], jnp.concatenate([before, after, jnp.zeros((6, width), F32)])


def modulate(rows, gain, shift_row):
    wide = rows.astype(F32)
    return wide * lax.rsqrt(jnp.mean(wide * wide, axis=-1, keepdims=True) + EPS) * gain + shift_row


def conv_block(value, length, taps, before, after):
    centre = value[:length]
    row = lax.broadcasted_iota(jnp.int32, centre.shape, 0)
    earlier = jnp.where(row == 0, before, pltpu.roll(centre, 1, 0))
    later = jnp.where(row == length - 1, after, pltpu.roll(centre, length - 1, 0))
    return silu(taps[0:1] * earlier + taps[1:2] * centre + taps[2:3] * later)


def column_blocks(widths):
    blocks = []
    for which, width in enumerate(widths):
        step = min(width, 256)
        blocks += [(which, at, step) for at in range(0, width, step)]
    return blocks


def rounded(value):
    return value.astype(BF16).astype(F32)


def recurrence_kernel(places, length, heads, latent, sp_count, *refs):
    refs = list(refs)
    pieces = [refs.pop(0) for _ in places]
    mods = refs.pop(0)
    halo = refs.pop(0) if latent else None
    gain, bias, decay_log, w_dt, taps_x, taps_b, w_x, w_b = refs[:8]
    refs = refs[8:]
    if latent:
        h, xs, bs, cum_out, cum_t_out, step_t_out = refs[:6]
        messages = refs[6:]
    else:
        states_out, h, xs, bs = refs
    blocks = column_blocks((w_x.shape[1], w_b.shape[1]))
    sp = lax.axis_index("sp")
    tp = lax.axis_index("tp")
    kind = 0 if latent else 1
    shift_row = mods[kind : kind + 1, :]
    gain_row = one_row(gain[...].astype(F32)) * (1.0 + mods[2 + kind : 3 + kind, :])
    for piece, (place, size, group) in zip(pieces, places):
        for at in range(0, piece.shape[0], 16):
            size_now = min(16, piece.shape[0] - at)
            offset = place(sp, tp, at)
            if not isinstance(offset, int):
                offset = pl.multiple_of(offset, 16)
            h[pl.ds(offset, size_now), :] = modulate(
                piece[at : at + size_now, :], gain_row, shift_row
            ).astype(BF16)
    if latent:
        edge = modulate(halo[...], gain_row, shift_row)
        pad = jnp.zeros((h.shape[0] - length - 8, edge.shape[1]), F32)
        h[length:, :] = jnp.concatenate([edge, pad], axis=0).astype(BF16)
    dt = rounded(jnp.dot(h[...], w_dt[...], preferred_element_type=F32))[:length]
    turn = lax.rem(LANES - tp * (2 * heads), LANES)
    dt = pltpu.roll(dt, turn, 1)
    filler = jnp.zeros((1, LANES - bias.shape[1]), F32)
    biased = dt + jnp.concatenate([bias[...], filler], axis=1)
    step = jnp.maximum(biased, 0.0) + jnp.log1p(jnp.exp(-jnp.abs(biased)))
    spent = step * jnp.exp(jnp.concatenate([decay_log[...], filler], axis=1))
    row = lax.broadcasted_iota(jnp.int32, (length, length), 0)
    col = lax.broadcasted_iota(jnp.int32, (length, length), 1)
    lower = jnp.where(row >= col, 1.0, 0.0).astype(F32)
    upper = jnp.where(row <= col, 1.0, 0.0).astype(F32)
    high = lax.Precision.HIGHEST
    prefix = jnp.dot(lower, spent, precision=high, preferred_element_type=F32)
    suffix = jnp.dot(upper, spent, precision=high, preferred_element_type=F32)
    lane = lax.broadcasted_iota(jnp.int32, (length, LANES), 1)
    cum = -jnp.where(lane % 2 == 0, prefix, suffix)
    total = jnp.where(lane[0:1] % 2 == 0, cum[length - 1 : length], cum[0:1])
    weight = jnp.exp(total - cum) * step
    if latent:
        cum_t = cum.T
        cum_out[...] = cum
        cum_t_out[...] = cum_t
        step_t_out[...] = step.T
        extra = messages[0].shape[0] - heads * HEAD_DIM
        rows = extra // 2
        ends = cum_t[0:rows]
        parity = lax.broadcasted_iota(jnp.int32, (rows, 1), 0) % 2
        ends = jnp.where(parity == 0, ends[:, length - 1 : length], ends[:, 0:1])
        decay = jnp.broadcast_to(jnp.exp(ends), (rows, LANES))
        decay_hi = decay.astype(BF16)
        decay_lo = (decay - decay_hi.astype(F32)).astype(BF16)
        for message in messages:
            message[heads * HEAD_DIM : heads * HEAD_DIM + rows, :] = decay_hi
            message[heads * HEAD_DIM + rows :, :] = decay_lo
        has_before = jnp.where(sp > 0, 1.0, 0.0)
        has_after = jnp.where(sp < sp_count - 1, 1.0, 0.0)
    for which, at, width in blocks:
        weights = (w_x, w_b)[which][:, at : at + width]
        value = rounded(jnp.dot(h[...], weights, preferred_element_type=F32))
        taps = (taps_x, taps_b)[which][:, at : at + width].astype(F32)
        if latent:
            before = value[length : length + 1] * has_before
            after = value[length + 1 : length + 2] * has_after
        else:
            before = after = 0.0
        out = conv_block(value, length, taps, before, after)
        (xs, bs)[which][:, at : at + width] = out.astype(BF16)
    state = w_b.shape[1] // heads
    for head in range(heads):
        mine = xs[:, head * HEAD_DIM : (head + 1) * HEAD_DIM].astype(F32)
        pair = jnp.concatenate(
            [mine * weight[:, 2 * head : 2 * head + 1], mine * weight[:, 2 * head + 1 : 2 * head + 2]],
            axis=1,
        ).astype(BF16)
        states = lax.dot_general(
            pair,
            bs[:, head * state : (head + 1) * state],
            (((0,), (0,)), ((), ())),
            preferred_element_type=F32,
        )
        if latent:
            for k, message in enumerate(messages, 1):
                forward = sp + k < sp_count
                chosen = jnp.where(forward, states[:HEAD_DIM], states[HEAD_DIM:])
                message[head * HEAD_DIM : (head + 1) * HEAD_DIM, :] = chosen.astype(BF16)
        else:
            states_out[head * 2 * HEAD_DIM : (head + 1) * 2 * HEAD_DIM, :] = states


def recurrence(places, pieces, length, heads, latent, mods, halo, common, sp_count):
    _, _, _, _, _, _, w_x, w_b = common
    depth = w_x.shape[0]
    state = w_b.shape[1] // heads
    struct = jax.ShapeDtypeStruct
    rows = length + 16 if latent else length
    if latent:
        extra = 2 * max(16, -(-2 * heads // 16) * 16)
        message = struct((heads * HEAD_DIM + extra, state), BF16)
        outs = [
            struct((rows, depth), BF16),
            struct((length, heads * HEAD_DIM), BF16),
            struct((length, heads * state), BF16),
            struct((length, LANES), F32),
            struct((LANES, length), F32),
            struct((LANES, length), F32),
        ] + [message] * (sp_count - 1)
        scratch = []
    else:
        outs = [struct((heads * 2 * HEAD_DIM, state), F32)]
        scratch = [
            pltpu.VMEM((rows, depth), BF16),
            pltpu.VMEM((length, heads * HEAD_DIM), BF16),
            pltpu.VMEM((length, heads * state), BF16),
        ]
    inputs = list(pieces) + [mods] + ([halo] if latent else []) + list(common)
    specs = [VMEM] * len(inputs)
    columns = w_x.shape[1] + w_b.shape[1]
    return call(
        functools.partial(recurrence_kernel, places, length, heads, latent, sp_count),
        outs,
        inputs,
        specs,
        scratch,
        flops=2 * rows * depth * columns,
        moved=2 * depth * columns,
    )


def outputs_kernel(length, heads, sp_count, *refs):
    h, xs, bs, cum, cum_t, step_t, taps_c, w_c, w_z, cs, y, zs = refs
    blocks = column_blocks((w_c.shape[1], w_z.shape[1]))
    sp = lax.axis_index("sp")
    has_before = jnp.where(sp > 0, 1.0, 0.0)
    has_after = jnp.where(sp < sp_count - 1, 1.0, 0.0)
    for which, at, width in blocks:
        weights = (w_c, w_z)[which][:, at : at + width]
        value = rounded(jnp.dot(h[...], weights, preferred_element_type=F32))
        if which == 0:
            before = value[length : length + 1] * has_before
            after = value[length + 1 : length + 2] * has_after
            taps = taps_c[:, at : at + width].astype(F32)
            cs[:, at : at + width] = conv_block(value, length, taps, before, after).astype(BF16)
        else:
            zs[:, at : at + width] = silu(value[:length])
    state = w_c.shape[1] // heads
    row = lax.broadcasted_iota(jnp.int32, (length, length), 0)
    col = lax.broadcasted_iota(jnp.int32, (length, length), 1)
    for head in range(heads):
        f, b = 2 * head, 2 * head + 1
        meet = lax.dot_general(
            cs[:, head * state : (head + 1) * state],
            bs[:, head * state : (head + 1) * state],
            (((1,), (1,)), ((), ())),
            preferred_element_type=F32,
        )
        span = jnp.where(
            row >= col,
            cum[:, f : f + 1] - cum_t[f : f + 1, :],
            cum[:, b : b + 1] - cum_t[b : b + 1, :],
        )
        ahead, behind = step_t[f : f + 1, :], step_t[b : b + 1, :]
        steps = jnp.where(row > col, ahead, jnp.where(row < col, behind, ahead + behind))
        mixed = (meet * jnp.exp(span) * steps).astype(BF16)
        y[:, head * HEAD_DIM : (head + 1) * HEAD_DIM] = jnp.dot(
            mixed, xs[:, head * HEAD_DIM : (head + 1) * HEAD_DIM], preferred_element_type=F32
        )


def block_outputs(heads, length, sp_count, h, xs, bs, cum, cum_t, step_t, taps_c, w_c, w_z):
    struct = jax.ShapeDtypeStruct
    depth = w_c.shape[0]
    columns = w_c.shape[1] + w_z.shape[1]
    return call(
        functools.partial(outputs_kernel, length, heads, sp_count),
        [
            struct((length, w_c.shape[1]), BF16),
            struct((length, w_z.shape[1]), F32),
            struct((length, w_z.shape[1]), F32),
        ],
        [h, xs, bs, cum, cum_t, step_t, taps_c, w_c, w_z],
        [VMEM] * 9,
        flops=2 * h.shape[0] * depth * columns,
        moved=2 * depth * columns,
    )


def finish_kernel(heads, sp_count, *refs):
    messages = refs[: sp_count - 1]
    ctx, cs, y, zs, cum, gain, out = refs[sp_count - 1 :]
    sp = lax.axis_index("sp")
    base = heads * HEAD_DIM
    rows = (messages[0].shape[0] - base) // 2
    decays = [
        m[base : base + rows, :].astype(F32) + m[base + rows :, :].astype(F32) for m in messages
    ]
    one = jnp.ones_like(decays[0])
    zero = jnp.zeros_like(decays[0])
    forward, backward = [None] * (sp_count - 1), [None] * (sp_count - 1)
    run = one
    for k in range(1, sp_count):
        active = k <= sp
        forward[k - 1] = jnp.where(active, run, zero)
        run = jnp.where(active, run * decays[k - 1], run)
    ctx_forward = run
    run = one
    for k in range(sp_count - 1, 0, -1):
        active = k > sp
        backward[k - 1] = jnp.where(active, run, zero)
        run = jnp.where(active, run * decays[k - 1], run)
    ctx_backward = run
    carry = jnp.exp(cum[...])
    gain_row = one_row(gain[...].astype(F32))
    state = cs.shape[1] // heads
    for head in range(heads):
        f, b = 2 * head, 2 * head + 1
        at = head * 2 * HEAD_DIM
        start_f = ctx[at : at + HEAD_DIM, :] * ctx_forward[f : f + 1]
        start_b = ctx[at + HEAD_DIM : at + 2 * HEAD_DIM, :] * ctx_backward[b : b + 1]
        for k in range(sp_count - 1):
            part = messages[k][head * HEAD_DIM : (head + 1) * HEAD_DIM, :].astype(F32)
            start_f = start_f + part * forward[k][f : f + 1]
            start_b = start_b + part * backward[k][b : b + 1]
        start = jnp.concatenate([start_f, start_b], axis=0).astype(BF16)
        carried = lax.dot_general(
            cs[:, head * state : (head + 1) * state],
            start,
            (((1,), (1,)), ((), ())),
            preferred_element_type=F32,
        )
        cols = slice(head * HEAD_DIM, (head + 1) * HEAD_DIM)
        total = (
            y[:, cols]
            + carried[:, :HEAD_DIM] * carry[:, f : f + 1]
            + carried[:, HEAD_DIM:] * carry[:, b : b + 1]
        )
        gated = total * zs[:, cols]
        scale = lax.rsqrt(jnp.mean(gated * gated, axis=-1, keepdims=True) + EPS)
        out[:, cols] = (gated * scale * gain_row[:, cols]).astype(BF16)


def finish(heads, sp_count, messages, ctx, cs, y, zs, cum, gain):
    inputs = list(messages) + [ctx, cs, y, zs, cum, gain]
    return call(
        functools.partial(finish_kernel, heads, sp_count),
        jax.ShapeDtypeStruct(y.shape, BF16),
        inputs,
        [VMEM] * len(inputs),
        flops=4 * y.size * 256,
        moved=8 * y.size,
    )


def project_out_kernel(count, *refs):
    pieces, w, *rest = refs[:count], *refs[count:]
    outs, acc = rest[:-1], rest[-1]
    tp = lax.axis_index("tp")
    total = None
    for q, piece in enumerate(pieces):
        depth = piece.shape[1]
        if count > 1:
            rows = w[pl.ds(pl.multiple_of((tp ^ q) * depth, depth), depth), :]
        else:
            rows = w[...]
        part = jnp.dot(piece[...], rows, preferred_element_type=F32)
        total = part if total is None else total + part
    acc[...] = total
    block = outs[0].shape[0]
    for q, out in enumerate(outs):
        at = pl.multiple_of((tp ^ q) * block, block) if count > 1 else 0
        out[...] = acc[pl.ds(at, block), :].astype(BF16)


def project_out(pieces, w):
    count = len(pieces)
    length = pieces[0].shape[0]
    width = w.shape[1]
    outs = [jax.ShapeDtypeStruct((length // count, width), BF16)] * count
    return call(
        functools.partial(project_out_kernel, count),
        outs,
        list(pieces) + [w],
        [VMEM] * (count + 1),
        [pltpu.VMEM((length, width), F32)],
        flops=2 * length * w.size,
        moved=2 * w.size,
    )


def residual_kernel(count, *refs):
    updates = refs[:count]
    latent, mods, out = refs[count:]
    tp = lax.axis_index("tp")
    for q, update in enumerate(updates):
        width = update.shape[1]
        cols = pl.ds(pl.multiple_of((tp ^ q) * width, width), width)
        gate = mods[4:5, cols]
        out[:, cols] = (latent[:, cols].astype(F32) + gate * update[...].astype(F32)).astype(BF16)


def residual(updates, latent, mods):
    return call(
        functools.partial(residual_kernel, len(updates)),
        jax.ShapeDtypeStruct(latent.shape, BF16),
        list(updates) + [latent, mods],
        [VMEM] * (len(updates) + 2),
    )


def layer(
    latent,
    context,
    cond,
    cond_ctx,
    mod_shift_w,
    mod_scale_w,
    mod_gate_w,
    norm_gain,
    proj_z,
    proj_x,
    proj_b,
    proj_c,
    proj_dt,
    conv_x,
    conv_b,
    conv_c,
    dt_bias,
    decay_log,
    head_gain,
    proj_out,
):
    sp_count, tp_count = lax.axis_size("sp"), lax.axis_size("tp")
    tp = lax.axis_index("tp")
    heads = proj_x.shape[1] // HEAD_DIM
    own, _ = latent.shape
    length = own * tp_count
    ctx_own = context.shape[0]
    ctx_length = ctx_own * sp_count
    fast = direct(tp_count)

    rows = exchange_tp(latent, 0)
    if fast:
        row_places = [
            ((lambda sp, tp, at, q=q: (tp ^ q) * own + at), own, None) for q in range(tp_count)
        ]
    else:
        row_places = [((lambda sp, tp, at: at), length, None)]

    up, down = mod_parts(cond, cond_ctx, latent, mod_shift_w, mod_scale_w, mod_gate_w)
    received = [shift(down if k == sp_count - 1 else up, "sp", k) for k in range(1, sp_count)]
    total = up[:8]
    for part in received:
        total = total + part[:8]
    edge = jnp.where(tp == 0, received[-1][8:], received[0][8:])
    payload = jnp.concatenate([total, edge], axis=0)
    mods, halo = assemble(exchange_tp(payload, 1, False), tp_count)

    if fast and ctx_own % 32 == 0:
        part = ctx_own // 2
        mine = lax.dynamic_slice_in_dim(context, (tp & 1) * part, part, 0)
        halves = [shift(mine, "sp", k) for k in range(1, sp_count)]
    else:
        halves = None

    common = (
        lane_rows(norm_gain),
        dt_bias[None],
        decay_log[None],
        proj_dt,
        conv_x,
        conv_b,
        proj_x,
        proj_b,
    )
    h, xs, bs, cum, cum_t, step_t, *messages = recurrence(
        row_places, rows, length, heads, True, mods, halo, common, sp_count
    )
    arrived = [shift(message, "sp", k) for k, message in enumerate(messages, 1)]
    if halves is not None:
        *halves, h = lax.optimization_barrier((*halves, h))
        ctx_pieces, ctx_places = [context], [((lambda sp, tp, at: sp * ctx_own + at), ctx_own, None)]
        for k, piece in enumerate(halves, 1):
            for bit, got in ((0, piece), (1, swap(piece, 1))):
                ctx_pieces.append(got)
                ctx_places.append(
                    (
                        lambda sp, tp, at, k=k, bit=bit: lax.rem(sp + sp_count - k, sp_count)
                        * ctx_own
                        + ((tp ^ bit) & 1) * part
                        + at,
                        part,
                        None,
                    )
                )
    else:
        ctx_pieces = [lax.all_gather(context, "sp", axis=0, tiled=True)]
        ctx_places = [((lambda sp, tp, at: at), ctx_length, None)]
    cs, y, zs = block_outputs(
        heads, length, sp_count, h, xs, bs, cum, cum_t, step_t, conv_c, proj_c, proj_z
    )
    mods_late, y = lax.optimization_barrier((mods, y))
    (ctx_states,) = recurrence(
        ctx_places, ctx_pieces, ctx_length, heads, False, mods_late, None, common, sp_count
    )
    mixed_heads = finish(heads, sp_count, arrived, ctx_states, cs, y, zs, cum, lane_rows(head_gain))
    updates = project_out(exchange_tp(mixed_heads, 1), proj_out)
    if fast:
        updates = [updates[0]] + [swap(updates[q], q) for q in range(1, tp_count)]
        return residual(updates, latent, mods)
    update = lax.all_to_all(updates[0], "tp", split_axis=0, concat_axis=1, tiled=True)
    update = lax.optimization_barrier(update).astype(F32)
    return (latent.astype(F32) + mods[4:5] * update).astype(BF16)


def solution(mesh):
    placed = (
        P(("sp", "tp"), None),
        P("sp", None),
        P("sp"),
        P("sp"),
        P("sp", "tp"),
        P("sp", "tp"),
        P("sp", "tp"),
        P(),
        P(None, "tp"),
        P(None, "tp"),
        P(None, "tp"),
        P(None, "tp"),
        P(),
        P(None, "tp"),
        P(None, "tp"),
        P(None, "tp"),
        P("tp"),
        P("tp"),
        P("tp"),
        P(None, "tp"),
    )
    return jax.shard_map(
        layer, mesh=mesh, in_specs=placed, out_specs=P(("sp", "tp"), None), check_vma=False
    )
```

profile of v0, /device:TPU:0, one launch (start us, length us, event | category | flops | bytes accessed | tf_op | source)
XLA Modules:
  0.0 107.7 jit_solution(8775821978910885946)
XLA Ops:
  0.0 3.1 %shard_map.190 = (f32[16,512]{1,0:T(8,128)}, f32[16,512]{1,0:T(8,128)}) custom-call(bf16[8,128]{1,0:T(8,128)(2,1)} %bitcast.15, bf16[8,128]{1,0:T(8,128)(2,1)} %bitcast.16, bf16[32,4096]{1,0:T(8,128)(2,1)} %refs_8_.5, bf16[1024,512]{1,0:T(8,128)(2,1)} %w_shift.1, bf16[1024,512]{1,0:T(8,128)(2,1)} %w_scale.1, bf16[1024,512]{1,0:T(8,128)(2,1)} %w_gate.1), custom_call_target="tpu_custom_call" | custom-call | flops 6291456 | bytes 3145728 | tf_op jit(solution)/shard_map/pallas_call | solution.py:38
  3.1 3.1 %collective-permute-start.7 = (f32[16,512]{1,0:T(8,128)}, f32[16,512]{1,0:T(8,128)S(1)}, u32[]{:S(2)}, u32[]{:S(2)}) collective-permute-start(f32[16,512]{1,0:T(8,128)} %get-tuple-element.35), channel_id=1, source_target_pairs={{0,8},{8,16},{16,24},{24,0},{1,9},{9,17},{17,25},{25,1},{2,10},{10... | collective-permute-start | bytes 98312 | tf_op jit(solution)/shard_map/ppermute | solution.py:51
  6.2 2.6 %collective-permute-start.8 = (f32[16,512]{1,0:T(8,128)}, f32[16,512]{1,0:T(8,128)S(1)}, u32[]{:S(2)}, u32[]{:S(2)}) collective-permute-start(f32[16,512]{1,0:T(8,128)} %get-tuple-element.35), channel_id=1, source_target_pairs={{0,16},{8,24},{16,0},{24,8},{1,17},{9,25},{17,1},{25,9},{2,18},{10... | collective-permute-start | bytes 98312 | tf_op jit(solution)/shard_map/ppermute | solution.py:51
  8.8 1.3 %collective-permute-start.9 = (f32[16,512]{1,0:T(8,128)}, f32[16,512]{1,0:T(8,128)S(1)}, u32[]{:S(2)}, u32[]{:S(2)}) collective-permute-start(f32[16,512]{1,0:T(8,128)} %get-tuple-element.36), channel_id=1, source_target_pairs={{0,24},{8,0},{16,8},{24,16},{1,25},{9,1},{17,9},{25,17},{2,26},{10... | collective-permute-start | bytes 98312 | tf_op jit(solution)/shard_map/ppermute | solution.py:51
  10.3 1.2 %collective-permute-done.8 = f32[16,512]{1,0:T(8,128)S(1)} collective-permute-done((f32[16,512]{1,0:T(8,128)}, f32[16,512]{1,0:T(8,128)S(1)}, u32[]{:S(2)}, u32[]{:S(2)}) %collective-permute-start.8) | collective-permute-done | bytes 32800 | tf_op jit(solution)/shard_map/ppermute | solution.py:51
  11.5 1.3 %collective-permute-done.9 = f32[16,512]{1,0:T(8,128)S(1)} collective-permute-done((f32[16,512]{1,0:T(8,128)}, f32[16,512]{1,0:T(8,128)S(1)}, u32[]{:S(2)}, u32[]{:S(2)}) %collective-permute-start.9) | collective-permute-done | bytes 32800 | tf_op jit(solution)/shard_map/ppermute | solution.py:51
  13.7 1.6 %collective-permute-start.11 = (f32[16,512]{1,0:T(8,128)S(1)}, f32[16,512]{1,0:T(8,128)S(1)}, u32[]{:S(2)}, u32[]{:S(2)}) collective-permute-start(f32[16,512]{1,0:T(8,128)S(1)} %pad_maximum_fusion.refs_0_), channel_id=1, source_target_pairs={{0,2},{1,3},{2,0},{3,1},{4,6},{5,7},{6,4},{7,5},{8,10},{9,11},{10,... | collective-permute-start | bytes 98312 | tf_op jit(solution)/shard_map/ppermute | solution.py:56
  15.5 1.5 %collective-permute-start.13 = (f32[16,512]{1,0:T(8,128)S(1)}, f32[16,512]{1,0:T(8,128)S(1)}, u32[]{:S(2)}, u32[]{:S(2)}) collective-permute-start(f32[16,512]{1,0:T(8,128)S(1)} %pad_maximum_fusion.refs_0_), channel_id=1, source_target_pairs={{0,4},{1,5},{2,6},{3,7},{4,0},{5,1},{6,2},{7,3},{8,12},{9,13},{10,... | collective-permute-start | bytes 98312 | tf_op jit(solution)/shard_map/ppermute | solution.py:56
  17.3 1.5 %collective-permute-start.1 = (bf16[32,4096]{1,0:T(8,128)(2,1)}, bf16[32,4096]{1,0:T(8,128)(2,1)S(1)}, u32[]{:S(2)}, u32[]{:S(2)}) collective-permute-start(bf16[32,4096]{1,0:T(8,128)(2,1)} %refs_8_.5), channel_id=1, source_target_pairs={{0,2},{1,3},{2,0},{3,1},{4,6},{5,7},{6,4},{7,5},{8,10},{9,11},{10,... | collective-permute-start | bytes 786440 | tf_op jit(solution)/shard_map/ppermute | solution.py:56
  18.7 1.5 %collective-permute-start.3 = (bf16[32,4096]{1,0:T(8,128)(2,1)}, bf16[32,4096]{1,0:T(8,128)(2,1)S(1)}, u32[]{:S(2)}, u32[]{:S(2)}) collective-permute-start(bf16[32,4096]{1,0:T(8,128)(2,1)} %refs_8_.5), channel_id=1, source_target_pairs={{0,4},{1,5},{2,6},{3,7},{4,0},{5,1},{6,2},{7,3},{8,12},{9,13},{10,... | collective-permute-start | bytes 786440 | tf_op jit(solution)/shard_map/ppermute | solution.py:56
  20.9 2.3 %collective-permute-start.15 = (f32[16,512]{1,0:T(8,128)S(1)}, f32[16,512]{1,0:T(8,128)S(1)}, u32[]{:S(2)}, u32[]{:S(2)}) collective-permute-start(f32[16,512]{1,0:T(8,128)S(1)} %pad_maximum_fusion.refs_0_), channel_id=1, source_target_pairs={{0,6},{1,7},{2,4},{3,5},{4,2},{5,3},{6,0},{7,1},{8,14},{9,15},{10,... | collective-permute-start | bytes 98312 | tf_op jit(solution)/shard_map/ppermute | solution.py:56
  23.2 1.1 %constant_dynamic-slice_fusion = bf16[32,4096]{1,0:T(8,128)(2,1)S(1)} fusion(bf16[64,4096]{1,0:T(8,128)(2,1)} %refs_0_.3, s32[]{:T(128)S(6)} %select_n.13), kind=kLoop, calls=%fused_computation.5 | loop fusion | bytes 524292 | tf_op jit(solution)/shard_map/dynamic_slice | solution.py:545
  24.4 9.4 %collective-permute-done.15.refs_6_ = f32[16,512]{1,0:T(8,128)S(1)} collective-permute-done((f32[16,512]{1,0:T(8,128)S(1)}, f32[16,512]{1,0:T(8,128)S(1)}, u32[]{:S(2)}, u32[]{:S(2)}) %collective-permute-start.15) | collective-permute-done | bytes 32800 | tf_op jit(solution)/shard_map/ppermute | solution.py:56
  35.6 2.9 %collective-permute-start.21 = (bf16[32,4096]{1,0:T(8,128)(2,1)S(1)}, bf16[32,4096]{1,0:T(8,128)(2,1)S(1)}, u32[]{:S(2)}, u32[]{:S(2)}) collective-permute-start(bf16[32,4096]{1,0:T(8,128)(2,1)S(1)} %constant_dynamic-slice_fusion), channel_id=1, source_target_pairs={{0,16},{8,24},{16,0},{24,8},{1,17},{9,25},{17,1},{25,9},{2,18},{10... | collective-permute-start | bytes 786440 | tf_op jit(solution)/shard_map/ppermute | solution.py:51
  39.4 7.9 %shard_map.192 = (bf16[272,4096]{1,0:T(8,128)(2,1)S(1)}, bf16[256,512]{1,0:T(8,128)(2,1)S(1)}, bf16[256,1024]{1,0:T(8,128)(2,1)S(1)}, f32[256,128]{1,0:T(8,128)S...) custom-call(bf16[32,4096]{1,0:T(8,128)(2,1)S(1)} %copy-done.5, ...), custom_call_target="tpu_custom_call" | custom-call | flops 3422552064 | bytes 12582912 | tf_op jit(solution)/shard_map/pallas_call | solution.py:38
  47.3 8.4 %collective-permute-done.21.refs_3_ = bf16[32,4096]{1,0:T(8,128)(2,1)S(1)} collective-permute-done((bf16[32,4096]{1,0:T(8,128)(2,1)S(1)}, bf16[32,4096]{1,0:T(8,128)(2,1)S(1)}, u32[]{:S(2)}, u32[]{:S(2)}) %collective-permute-start.21) | collective-permute-done | bytes 262176 | tf_op jit(solution)/shard_map/ppermute | solution.py:51
  56.2 5.2 %shard_map.193 = (bf16[256,1024]{1,0:T(8,128)(2,1)S(1)}, f32[256,512]{1,0:T(8,128)S(1)}, f32[256,512]{1,0:T(8,128)S(1)}) custom-call(bf16[272,4096]{1,0:T(8,128)(2,1)S(1)} %get-tuple-element.46.refs_0_, bf16[256,512]{1,0:T(8,128)(2,1)S(1)} %get-tuple-element.47.refs_1_, bf16[256,1024]{1,0:T(8,128)(2,1)S(1)} %get-tuple-element.48.refs_2_, ...), custom_call_target="tpu_custom_call" | custom-call | flops 3422552064 | bytes 12582912 | tf_op jit(solution)/shard_map/pallas_call | solution.py:38
  61.5 6.2 %collective-permute-start.17 = (bf16[544,128]{1,0:T(8,128)(2,1)S(1)}, bf16[544,128]{1,0:T(8,128)(2,1)S(1)}, u32[]{:S(2)}, u32[]{:S(2)}) collective-permute-start(bf16[544,128]{1,0:T(8,128)(2,1)S(1)} %get-tuple-element.39), channel_id=1, source_target_pairs={{0,8},{8,16},{16,24},{24,0},{1,9},{9,17},{17,25},{25,1},{2,10},{10... | collective-permute-start | bytes 417800 | tf_op jit(solution)/shard_map/ppermute | solution.py:51
  67.7 2.4 %collective-permute-start.19 = (bf16[544,128]{1,0:T(8,128)(2,1)S(1)}, bf16[544,128]{1,0:T(8,128)(2,1)S(1)}, u32[]{:S(2)}, u32[]{:S(2)}) collective-permute-start(bf16[544,128]{1,0:T(8,128)(2,1)S(1)} %get-tuple-element.41), channel_id=1, source_target_pairs={{0,24},{8,0},{16,8},{24,16},{1,25},{9,1},{17,9},{25,17},{2,26},{10... | collective-permute-start | bytes 417800 | tf_op jit(solution)/shard_map/ppermute | solution.py:51
  70.2 7.2 %shard_map.194.refs_3_ = f32[1024,128]{1,0:T(8,128)S(1)} custom-call(bf16[64,4096]{1,0:T(8,128)(2,1)S(1)} %copy-done.6, bf16[32,4096]{1,0:T(8,128)(2,1)S(1)} %collective-permute-done.20.refs_1_, bf16[32,4096]{1,0:T(8,128)(2,1)S(1)} %collective-permute-done.23.refs_2_, bf16[32,4096]{1,0:T(8,128)(2,1)S(1)} %collective-permute-done.21.refs_3_, ...), custom_call_target="tpu_custom_call" | custom-call | flops 3221225472 | bytes 12582912 | tf_op jit(solution)/shard_map/pallas_call | solution.py:38
  77.5 2.2 %shard_map.195.refs_0_ = bf16[256,512]{1,0:T(8,128)(2,1)S(1)} custom-call(bf16[544,128]{1,0:T(8,128)(2,1)S(1)} %collective-permute-done.17.refs_0_, bf16[544,128]{1,0:T(8,128)(2,1)S(1)} %collective-permute-done.18.refs_1_, bf16[544,128]{1,0:T(8,128)(2,1)S(1)} %collective-permute-done.19.refs_2_, f32[1024,128]{1,0:T(8,128)S(1)} %shard_map.194.refs_3_, ...), custom_call_target="tpu_custom_call" | custom-call | flops 134217728 | bytes 1048576 | tf_op jit(solution)/shard_map/pallas_call | solution.py:38
  79.6 1.4 %collective-permute-start.27 = (bf16[256,512]{1,0:T(8,128)(2,1)S(1)}, bf16[256,512]{1,0:T(8,128)(2,1)S(1)}, u32[]{:S(2)}, u32[]{:S(2)}) collective-permute-start(bf16[256,512]{1,0:T(8,128)(2,1)S(1)} %shard_map.195.refs_0_), channel_id=1, source_target_pairs={{0,2},{1,3},{2,0},{3,1},{4,6},{5,7},{6,4},{7,5},{8,10},{9,11},{10,... | collective-permute-start | bytes 786440 | tf_op jit(solution)/shard_map/ppermute | solution.py:56
  81.7 1.5 %collective-permute-start.31 = (bf16[256,512]{1,0:T(8,128)(2,1)S(1)}, bf16[256,512]{1,0:T(8,128)(2,1)S(1)}, u32[]{:S(2)}, u32[]{:S(2)}) collective-permute-start(bf16[256,512]{1,0:T(8,128)(2,1)S(1)} %shard_map.195.refs_0_), channel_id=1, source_target_pairs={{0,6},{1,7},{2,4},{3,5},{4,2},{5,3},{6,0},{7,1},{8,14},{9,15},{10,... | collective-permute-start | bytes 786440 | tf_op jit(solution)/shard_map/ppermute | solution.py:56
  83.2 5.7 %collective-permute-done.27.refs_2_ = bf16[256,512]{1,0:T(8,128)(2,1)S(1)} collective-permute-done((bf16[256,512]{1,0:T(8,128)(2,1)S(1)}, bf16[256,512]{1,0:T(8,128)(2,1)S(1)}, u32[]{:S(2)}, u32[]{:S(2)}) %collective-permute-start.27) | collective-permute-done | bytes 262176 | tf_op jit(solution)/shard_map/ppermute | solution.py:56
  88.9 5.7 %collective-permute-done.29.refs_4_ = bf16[256,512]{1,0:T(8,128)(2,1)S(1)} collective-permute-done((bf16[256,512]{1,0:T(8,128)(2,1)S(1)}, bf16[256,512]{1,0:T(8,128)(2,1)S(1)}, u32[]{:S(2)}, u32[]{:S(2)}) %collective-permute-start.29) | collective-permute-done | bytes 262176 | tf_op jit(solution)/shard_map/ppermute | solution.py:56
  95.1 1.0 collective-permute-done.30.refs_5_
  96.5 1.3 %shard_map.196 = (bf16[32,512]{1,0:T(8,128)(2,1)S(1)}, bf16[32,512]{1,0:T(8,128)(2,1)S(1)}, bf16[32,512]{1,0:T(8,128)(2,1)S(1)}, bf16[32,512]{1,0:T(8,128)(2,1)S...) custom-call(bf16[256,512]{1,0:T(8,128)(2,1)S(1)} %shard_map.195.refs, ...), custom_call_target="tpu_custom_call" | custom-call | flops 1073741824 | bytes 4194304 | tf_op jit(solution)/shard_map/pallas_call | solution.py:38
  98.6 1.1 %collective-permute-start.35 = (bf16[32,512]{1,0:T(8,128)(2,1)S(1)}, bf16[32,512]{1,0:T(8,128)(2,1)S(1)}, u32[]{:S(2)}, u32[]{:S(2)}) collective-permute-start(bf16[32,512]{1,0:T(8,128)(2,1)S(1)} %get-tuple-element.60), channel_id=1, source_target_pairs={{0,3},{1,2},{2,1},{3,0},{4,7},{5,6},{6,5},{7,4},{8,11},{9,10},{10,... | collective-permute-start | bytes 98312 | tf_op jit(solution)/shard_map/ppermute | solution.py:56
  100.3 1.2 %collective-permute-start.37 = (bf16[32,512]{1,0:T(8,128)(2,1)S(1)}, bf16[32,512]{1,0:T(8,128)(2,1)S(1)}, u32[]{:S(2)}, u32[]{:S(2)}) collective-permute-start(bf16[32,512]{1,0:T(8,128)(2,1)S(1)} %get-tuple-element.62), channel_id=1, source_target_pairs={{0,5},{1,4},{2,7},{3,6},{4,1},{5,0},{6,3},{7,2},{8,13},{9,12},{10,... | collective-permute-start | bytes 98312 | tf_op jit(solution)/shard_map/ppermute | solution.py:56
  101.5 0.8 collective-permute-start.38
  102.3 1.8 %collective-permute-start.39 = (bf16[32,512]{1,0:T(8,128)(2,1)S(1)}, bf16[32,512]{1,0:T(8,128)(2,1)S(1)}, u32[]{:S(2)}, u32[]{:S(2)}) collective-permute-start(bf16[32,512]{1,0:T(8,128)(2,1)S(1)} %get-tuple-element.64), channel_id=1, source_target_pairs={{0,7},{1,6},{2,5},{3,4},{4,3},{5,2},{6,1},{7,0},{8,15},{9,14},{10,... | collective-permute-start | bytes 98312 | tf_op jit(solution)/shard_map/ppermute | solution.py:56
  104.1 2.3 %collective-permute-done.38.refs_6_ = bf16[32,512]{1,0:T(8,128)(2,1)S(1)} collective-permute-done((bf16[32,512]{1,0:T(8,128)(2,1)S(1)}, bf16[32,512]{1,0:T(8,128)(2,1)S(1)}, u32[]{:S(2)}, u32[]{:S(2)}) %collective-permute-start.38) | collective-permute-done | bytes 32800 | tf_op jit(solution)/shard_map/ppermute | solution.py:56
  (92 shorter events, 9.6 us)
Async XLA Ops:
  3.1 7.2 %collective-permute-start.7 = (f32[16,512]{1,0:T(8,128)}, f32[16,512]{1,0:T(8,128)S(1)}, u32[]{:S(2)}, u32[]{:S(2)}) collective-permute-start(f32[16,512]{1,0:T(8,128)} %get-tuple-element.35), channel_id=1, source_target_pairs={{0,8},{8,16},{16,24},{24,0},{1,9},{9,17},{17,25},{25,1},{2,10},{10... | collective-permute-start | bytes 98312 | tf_op jit(solution)/shard_map/ppermute | solution.py:51
  6.2 5.4 %collective-permute-start.8 = (f32[16,512]{1,0:T(8,128)}, f32[16,512]{1,0:T(8,128)S(1)}, u32[]{:S(2)}, u32[]{:S(2)}) collective-permute-start(f32[16,512]{1,0:T(8,128)} %get-tuple-element.35), channel_id=1, source_target_pairs={{0,16},{8,24},{16,0},{24,8},{1,17},{9,25},{17,1},{25,9},{2,18},{10... | collective-permute-start | bytes 98312 | tf_op jit(solution)/shard_map/ppermute | solution.py:51
  13.7 5.1 %collective-permute-start.11 = (f32[16,512]{1,0:T(8,128)S(1)}, f32[16,512]{1,0:T(8,128)S(1)}, u32[]{:S(2)}, u32[]{:S(2)}) collective-permute-start(f32[16,512]{1,0:T(8,128)S(1)} %pad_maximum_fusion.refs_0_), channel_id=1, source_target_pairs={{0,2},{1,3},{2,0},{3,1},{4,6},{5,7},{6,4},{7,5},{8,10},{9,11},{10,... | collective-permute-start | bytes 98312 | tf_op jit(solution)/shard_map/ppermute | solution.py:56
  15.2 5.0 %collective-permute-start.12 = (f32[16,512]{1,0:T(8,128)S(1)}, f32[16,512]{1,0:T(8,128)S(1)}, u32[]{:S(2)}, u32[]{:S(2)}) collective-permute-start(f32[16,512]{1,0:T(8,128)S(1)} %pad_maximum_fusion.refs_0_), channel_id=1, source_target_pairs={{0,3},{1,2},{2,1},{3,0},{4,7},{5,6},{6,5},{7,4},{8,11},{9,10},{10,... | collective-permute-start | bytes 98312 | tf_op jit(solution)/shard_map/ppermute | solution.py:56
  15.5 5.4 %collective-permute-start.13 = (f32[16,512]{1,0:T(8,128)S(1)}, f32[16,512]{1,0:T(8,128)S(1)}, u32[]{:S(2)}, u32[]{:S(2)}) collective-permute-start(f32[16,512]{1,0:T(8,128)S(1)} %pad_maximum_fusion.refs_0_), channel_id=1, source_target_pairs={{0,4},{1,5},{2,6},{3,7},{4,0},{5,1},{6,2},{7,3},{8,12},{9,13},{10,... | collective-permute-start | bytes 98312 | tf_op jit(solution)/shard_map/ppermute | solution.py:56
  17.1 6.1 %collective-permute-start.14 = (f32[16,512]{1,0:T(8,128)S(1)}, f32[16,512]{1,0:T(8,128)S(1)}, u32[]{:S(2)}, u32[]{:S(2)}) collective-permute-start(f32[16,512]{1,0:T(8,128)S(1)} %pad_maximum_fusion.refs_0_), channel_id=1, source_target_pairs={{0,5},{1,4},{2,7},{3,6},{4,1},{5,0},{6,3},{7,2},{8,13},{9,12},{10,... | collective-permute-start | bytes 98312 | tf_op jit(solution)/shard_map/ppermute | solution.py:56
  17.3 16.8 %collective-permute-start.1 = (bf16[32,4096]{1,0:T(8,128)(2,1)}, bf16[32,4096]{1,0:T(8,128)(2,1)S(1)}, u32[]{:S(2)}, u32[]{:S(2)}) collective-permute-start(bf16[32,4096]{1,0:T(8,128)(2,1)} %refs_8_.5), channel_id=1, source_target_pairs={{0,2},{1,3},{2,0},{3,1},{4,6},{5,7},{6,4},{7,5},{8,10},{9,11},{10,... | collective-permute-start | bytes 786440 | tf_op jit(solution)/shard_map/ppermute | solution.py:56
  18.7 15.7 %collective-permute-start.3 = (bf16[32,4096]{1,0:T(8,128)(2,1)}, bf16[32,4096]{1,0:T(8,128)(2,1)S(1)}, u32[]{:S(2)}, u32[]{:S(2)}) collective-permute-start(bf16[32,4096]{1,0:T(8,128)(2,1)} %refs_8_.5), channel_id=1, source_target_pairs={{0,4},{1,5},{2,6},{3,7},{4,0},{5,1},{6,2},{7,3},{8,12},{9,13},{10,... | collective-permute-start | bytes 786440 | tf_op jit(solution)/shard_map/ppermute | solution.py:56
  20.3 14.3 %collective-permute-start.5 = (bf16[32,4096]{1,0:T(8,128)(2,1)}, bf16[32,4096]{1,0:T(8,128)(2,1)S(1)}, u32[]{:S(2)}, u32[]{:S(2)}) collective-permute-start(bf16[32,4096]{1,0:T(8,128)(2,1)} %refs_8_.5), channel_id=1, source_target_pairs={{0,6},{1,7},{2,4},{3,5},{4,2},{5,3},{6,0},{7,1},{8,14},{9,15},{10,... | collective-permute-start | bytes 786440 | tf_op jit(solution)/shard_map/ppermute | solution.py:56
  20.9 12.9 %collective-permute-start.15 = (f32[16,512]{1,0:T(8,128)S(1)}, f32[16,512]{1,0:T(8,128)S(1)}, u32[]{:S(2)}, u32[]{:S(2)}) collective-permute-start(f32[16,512]{1,0:T(8,128)S(1)} %pad_maximum_fusion.refs_0_), channel_id=1, source_target_pairs={{0,6},{1,7},{2,4},{3,5},{4,2},{5,3},{6,0},{7,1},{8,14},{9,15},{10,... | collective-permute-start | bytes 98312 | tf_op jit(solution)/shard_map/ppermute | solution.py:56
  23.2 10.6 %collective-permute-start.16 = (f32[16,512]{1,0:T(8,128)S(1)}, f32[16,512]{1,0:T(8,128)S(1)}, u32[]{:S(2)}, u32[]{:S(2)}) collective-permute-start(f32[16,512]{1,0:T(8,128)S(1)} %pad_maximum_fusion.refs_0_), channel_id=1, source_target_pairs={{0,7},{1,6},{2,5},{3,4},{4,3},{5,2},{6,1},{7,0},{8,15},{9,14},{10,... | collective-permute-start | bytes 98312 | tf_op jit(solution)/shard_map/ppermute | solution.py:56
  33.8 13.4 %collective-permute-start.20 = (bf16[32,4096]{1,0:T(8,128)(2,1)S(1)}, bf16[32,4096]{1,0:T(8,128)(2,1)S(1)}, u32[]{:S(2)}, u32[]{:S(2)}) collective-permute-start(bf16[32,4096]{1,0:T(8,128)(2,1)S(1)} %constant_dynamic-slice_fusion), channel_id=1, source_target_pairs={{0,8},{8,16},{16,24},{24,0},{1,9},{9,17},{17,25},{25,1},{2,10},{10... | collective-permute-start | bytes 786440 | tf_op jit(solution)/shard_map/ppermute | solution.py:51
  34.1 4.4 %collective-permute-start.2 = (bf16[32,4096]{1,0:T(8,128)(2,1)S(1)}, bf16[32,4096]{1,0:T(8,128)(2,1)S(1)}, u32[]{:S(2)}, u32[]{:S(2)}) collective-permute-start(bf16[32,4096]{1,0:T(8,128)(2,1)S(1)} %collective-permute-done.1.refs_2_), channel_id=1, source_target_pairs={{0,1},{1,0},{2,3},{3,2},{4,5},{5,4},{6,7},{7,6},{8,9},{9,8},{10,11... | collective-permute-start | bytes 786440 | tf_op jit(solution)/shard_map/ppermute | solution.py:56
  34.4 4.8 %collective-permute-start.4 = (bf16[32,4096]{1,0:T(8,128)(2,1)S(1)}, bf16[32,4096]{1,0:T(8,128)(2,1)S(1)}, u32[]{:S(2)}, u32[]{:S(2)}) collective-permute-start(bf16[32,4096]{1,0:T(8,128)(2,1)S(1)} %collective-permute-done.3.refs_4_), channel_id=1, source_target_pairs={{0,1},{1,0},{2,3},{3,2},{4,5},{5,4},{6,7},{7,6},{8,9},{9,8},{10,11... | collective-permute-start | bytes 786440 | tf_op jit(solution)/shard_map/ppermute | solution.py:56
  34.6 4.6 %collective-permute-start.6 = (bf16[32,4096]{1,0:T(8,128)(2,1)S(1)}, bf16[32,4096]{1,0:T(8,128)(2,1)S(1)}, u32[]{:S(2)}, u32[]{:S(2)}) collective-permute-start(bf16[32,4096]{1,0:T(8,128)(2,1)S(1)} %collective-permute-done.5.refs_6_), channel_id=1, source_target_pairs={{0,1},{1,0},{2,3},{3,2},{4,5},{5,4},{6,7},{7,6},{8,9},{9,8},{10,11... | collective-permute-start | bytes 786440 | tf_op jit(solution)/shard_map/ppermute | solution.py:56
  35.6 20.1 %collective-permute-start.21 = (bf16[32,4096]{1,0:T(8,128)(2,1)S(1)}, bf16[32,4096]{1,0:T(8,128)(2,1)S(1)}, u32[]{:S(2)}, u32[]{:S(2)}) collective-permute-start(bf16[32,4096]{1,0:T(8,128)(2,1)S(1)} %constant_dynamic-slice_fusion), channel_id=1, source_target_pairs={{0,16},{8,24},{16,0},{24,8},{1,17},{9,25},{17,1},{25,9},{2,18},{10... | collective-permute-start | bytes 786440 | tf_op jit(solution)/shard_map/ppermute | solution.py:51
  38.5 17.2 %collective-permute-start.22 = (bf16[32,4096]{1,0:T(8,128)(2,1)S(1)}, bf16[32,4096]{1,0:T(8,128)(2,1)S(1)}, u32[]{:S(2)}, u32[]{:S(2)}) collective-permute-start(bf16[32,4096]{1,0:T(8,128)(2,1)S(1)} %constant_dynamic-slice_fusion), channel_id=1, source_target_pairs={{0,24},{8,0},{16,8},{24,16},{1,25},{9,1},{17,9},{25,17},{2,26},{10... | collective-permute-start | bytes 786440 | tf_op jit(solution)/shard_map/ppermute | solution.py:51
  55.7 12.1 %collective-permute-start.23 = (bf16[32,4096]{1,0:T(8,128)(2,1)S(1)}, bf16[32,4096]{1,0:T(8,128)(2,1)S(1)}, u32[]{:S(2)}, u32[]{:S(2)}) collective-permute-start(bf16[32,4096]{1,0:T(8,128)(2,1)S(1)} %collective-permute-done.20.refs_1_), channel_id=1, source_target_pairs={{0,1},{1,0},{2,3},{3,2},{4,5},{5,4},{6,7},{7,6},{8,9},{9,8},{10,11... | collective-permute-start | bytes 786440 | tf_op jit(solution)/shard_map/ppermute | solution.py:56
  55.7 14.5 %collective-permute-start.24 = (bf16[32,4096]{1,0:T(8,128)(2,1)S(1)}, bf16[32,4096]{1,0:T(8,128)(2,1)S(1)}, u32[]{:S(2)}, u32[]{:S(2)}) collective-permute-start(bf16[32,4096]{1,0:T(8,128)(2,1)S(1)} %collective-permute-done.21.refs_3_), channel_id=1, source_target_pairs={{0,1},{1,0},{2,3},{3,2},{4,5},{5,4},{6,7},{7,6},{8,9},{9,8},{10,11... | collective-permute-start | bytes 786440 | tf_op jit(solution)/shard_map/ppermute | solution.py:56
  56.2 14.0 %collective-permute-start.25 = (bf16[32,4096]{1,0:T(8,128)(2,1)S(1)}, bf16[32,4096]{1,0:T(8,128)(2,1)S(1)}, u32[]{:S(2)}, u32[]{:S(2)}) collective-permute-start(bf16[32,4096]{1,0:T(8,128)(2,1)S(1)} %collective-permute-done.22.refs_5_), channel_id=1, source_target_pairs={{0,1},{1,0},{2,3},{3,2},{4,5},{5,4},{6,7},{7,6},{8,9},{9,8},{10,11... | collective-permute-start | bytes 786440 | tf_op jit(solution)/shard_map/ppermute | solution.py:56
  61.5 15.9 %collective-permute-start.17 = (bf16[544,128]{1,0:T(8,128)(2,1)S(1)}, bf16[544,128]{1,0:T(8,128)(2,1)S(1)}, u32[]{:S(2)}, u32[]{:S(2)}) collective-permute-start(bf16[544,128]{1,0:T(8,128)(2,1)S(1)} %get-tuple-element.39), channel_id=1, source_target_pairs={{0,8},{8,16},{16,24},{24,0},{1,9},{9,17},{17,25},{25,1},{2,10},{10... | collective-permute-start | bytes 417800 | tf_op jit(solution)/shard_map/ppermute | solution.py:51
  67.7 9.7 %collective-permute-start.18 = (bf16[544,128]{1,0:T(8,128)(2,1)S(1)}, bf16[544,128]{1,0:T(8,128)(2,1)S(1)}, u32[]{:S(2)}, u32[]{:S(2)}) collective-permute-start(bf16[544,128]{1,0:T(8,128)(2,1)S(1)} %get-tuple-element.40), channel_id=1, source_target_pairs={{0,16},{8,24},{16,0},{24,8},{1,17},{9,25},{17,1},{25,9},{2,18},{10... | collective-permute-start | bytes 417800 | tf_op jit(solution)/shard_map/ppermute | solution.py:51
  67.7 9.7 %collective-permute-start.19 = (bf16[544,128]{1,0:T(8,128)(2,1)S(1)}, bf16[544,128]{1,0:T(8,128)(2,1)S(1)}, u32[]{:S(2)}, u32[]{:S(2)}) collective-permute-start(bf16[544,128]{1,0:T(8,128)(2,1)S(1)} %get-tuple-element.41), channel_id=1, source_target_pairs={{0,24},{8,0},{16,8},{24,16},{1,25},{9,1},{17,9},{25,17},{2,26},{10... | collective-permute-start | bytes 417800 | tf_op jit(solution)/shard_map/ppermute | solution.py:51
  79.6 9.2 %collective-permute-start.27 = (bf16[256,512]{1,0:T(8,128)(2,1)S(1)}, bf16[256,512]{1,0:T(8,128)(2,1)S(1)}, u32[]{:S(2)}, u32[]{:S(2)}) collective-permute-start(bf16[256,512]{1,0:T(8,128)(2,1)S(1)} %shard_map.195.refs_0_), channel_id=1, source_target_pairs={{0,2},{1,3},{2,0},{3,1},{4,6},{5,7},{6,4},{7,5},{8,10},{9,11},{10,... | collective-permute-start | bytes 786440 | tf_op jit(solution)/shard_map/ppermute | solution.py:56
  81.1 13.5 %collective-permute-start.29 = (bf16[256,512]{1,0:T(8,128)(2,1)S(1)}, bf16[256,512]{1,0:T(8,128)(2,1)S(1)}, u32[]{:S(2)}, u32[]{:S(2)}) collective-permute-start(bf16[256,512]{1,0:T(8,128)(2,1)S(1)} %shard_map.195.refs_0_), channel_id=1, source_target_pairs={{0,4},{1,5},{2,6},{3,7},{4,0},{5,1},{6,2},{7,3},{8,12},{9,13},{10,... | collective-permute-start | bytes 786440 | tf_op jit(solution)/shard_map/ppermute | solution.py:56
  81.7 12.9 %collective-permute-start.31 = (bf16[256,512]{1,0:T(8,128)(2,1)S(1)}, bf16[256,512]{1,0:T(8,128)(2,1)S(1)}, u32[]{:S(2)}, u32[]{:S(2)}) collective-permute-start(bf16[256,512]{1,0:T(8,128)(2,1)S(1)} %shard_map.195.refs_0_), channel_id=1, source_target_pairs={{0,6},{1,7},{2,4},{3,5},{4,2},{5,3},{6,0},{7,1},{8,14},{9,15},{10,... | collective-permute-start | bytes 786440 | tf_op jit(solution)/shard_map/ppermute | solution.py:56
  83.2 11.9 %collective-permute-start.26 = (bf16[256,512]{1,0:T(8,128)(2,1)S(1)}, bf16[256,512]{1,0:T(8,128)(2,1)S(1)}, u32[]{:S(2)}, u32[]{:S(2)}) collective-permute-start(bf16[256,512]{1,0:T(8,128)(2,1)S(1)} %shard_map.195.refs_0_), channel_id=1, source_target_pairs={{0,1},{1,0},{2,3},{3,2},{4,5},{5,4},{6,7},{7,6},{8,9},{9,8},{10,11... | collective-permute-start | bytes 786440 | tf_op jit(solution)/shard_map/ppermute | solution.py:56
  88.9 6.2 %collective-permute-start.28 = (bf16[256,512]{1,0:T(8,128)(2,1)S(1)}, bf16[256,512]{1,0:T(8,128)(2,1)S(1)}, u32[]{:S(2)}, u32[]{:S(2)}) collective-permute-start(bf16[256,512]{1,0:T(8,128)(2,1)S(1)} %collective-permute-done.27.refs_2_), channel_id=1, source_target_pairs={{0,1},{1,0},{2,3},{3,2},{4,5},{5,4},{6,7},{7,6},{8,9},{9,8},{10,11... | collective-permute-start | bytes 786440 | tf_op jit(solution)/shard_map/ppermute | solution.py:56
  98.6 5.5 %collective-permute-start.35 = (bf16[32,512]{1,0:T(8,128)(2,1)S(1)}, bf16[32,512]{1,0:T(8,128)(2,1)S(1)}, u32[]{:S(2)}, u32[]{:S(2)}) collective-permute-start(bf16[32,512]{1,0:T(8,128)(2,1)S(1)} %get-tuple-element.60), channel_id=1, source_target_pairs={{0,3},{1,2},{2,1},{3,0},{4,7},{5,6},{6,5},{7,4},{8,11},{9,10},{10,... | collective-permute-start | bytes 98312 | tf_op jit(solution)/shard_map/ppermute | solution.py:56
  99.7 4.4 %collective-permute-start.36 = (bf16[32,512]{1,0:T(8,128)(2,1)S(1)}, bf16[32,512]{1,0:T(8,128)(2,1)S(1)}, u32[]{:S(2)}, u32[]{:S(2)}) collective-permute-start(bf16[32,512]{1,0:T(8,128)(2,1)S(1)} %get-tuple-element.61), channel_id=1, source_target_pairs={{0,4},{1,5},{2,6},{3,7},{4,0},{5,1},{6,2},{7,3},{8,12},{9,13},{10,... | collective-permute-start | bytes 98312 | tf_op jit(solution)/shard_map/ppermute | solution.py:56
  101.5 4.9 %collective-permute-start.38 = (bf16[32,512]{1,0:T(8,128)(2,1)S(1)}, bf16[32,512]{1,0:T(8,128)(2,1)S(1)}, u32[]{:S(2)}, u32[]{:S(2)}) collective-permute-start(bf16[32,512]{1,0:T(8,128)(2,1)S(1)} %get-tuple-element.63), channel_id=1, source_target_pairs={{0,6},{1,7},{2,4},{3,5},{4,2},{5,3},{6,0},{7,1},{8,14},{9,15},{10,... | collective-permute-start | bytes 98312 | tf_op jit(solution)/shard_map/ppermute | solution.py:56
  102.3 4.6 %collective-permute-start.39 = (bf16[32,512]{1,0:T(8,128)(2,1)S(1)}, bf16[32,512]{1,0:T(8,128)(2,1)S(1)}, u32[]{:S(2)}, u32[]{:S(2)}) collective-permute-start(bf16[32,512]{1,0:T(8,128)(2,1)S(1)} %get-tuple-element.64), channel_id=1, source_target_pairs={{0,7},{1,6},{2,5},{3,4},{4,3},{5,2},{6,1},{7,0},{8,15},{9,14},{10,... | collective-permute-start | bytes 98312 | tf_op jit(solution)/shard_map/ppermute | solution.py:56
  (24 other events, 275.3 us)
where the time goes:
time: 109 us; the launch traced here: 108 us
  starting transfers between devices  40.9 us (38%)
  waiting for transfers between devices  36.8 us (34%)
  Pallas kernels  27.8 us (26%)
  local copies, waits for them, and re-layouts  1.22 us (1%)
    pallas_call x8, Pallas kernels, call(): pl.pallas_call(kernel, out_shape=outs, in_specs=specs, out_specs=jax.tree...  27.8 us
    ppermute x31, waiting for transfers between devices, swap(): return lax.ppermute(array, 'tp', [(i, i ^ bits) for i in range(count)])  25.5 us
    ppermute x31, starting transfers between devices, swap(): return lax.ppermute(array, 'tp', [(i, i ^ bits) for i in range(count)])  21.4 us
    ppermute x9, starting transfers between devices, shift(): lax.ppermute(array, axis, [(i, (i + step) % count) for i in range(count)])  19.5 us
    ppermute x9, waiting for transfers between devices, shift(): lax.ppermute(array, axis, [(i, (i + step) % count) for i in range(count)])  11.2 us
  transfers between devices with their start and end apart: 40, of which 13 were waited for; matrix products, arithmetic and copies ran while one was open for 1% of the time, Pallas kernels for 19%

commit v1 on v0

--- a/solution.py
+++ b/solution.py
@@ -65,13 +65,12 @@
     if not direct(count):
         return [lax.all_gather(array, "tp", axis=dim, tiled=True)]
     pieces = [array] + [None] * (count - 1)
+    if not relay:
+        return [array] + [swap(array, q) for q in range(1, count)]
     for q in range(2, count, 2):
         pieces[q] = swap(array, q)
     for q in range(0, count, 2):
-        if relay:
-            pieces[q + 1] = swap(pieces[q], 1)
-        else:
-            pieces[q + 1] = swap(array, q + 1)
+        pieces[q + 1] = swap(pieces[q], 1)
     return pieces
 
 
@@ -83,7 +82,10 @@
     return jnp.concatenate([rows[i : i + 1, :] for i in range(rows.shape[0])], axis=1)
 
 
-def mod_kernel(cond, cond_ctx, rows, w_shift, w_scale, w_gate, up, down):
+def mod_kernel(cond, cond_ctx, rows, context, w_shift, w_scale, w_gate, up, down, mine):
+    part = mine.shape[0]
+    core = lax.axis_index("tp") & 1
+    mine[...] = context[pl.ds(pl.multiple_of(core * part, part), part), :]
     width = w_shift.shape[1]
     acts = [silu(one_row(c[...].astype(F32))) for c in (cond, cond_ctx)]
     both = jnp.concatenate(acts, axis=0).astype(BF16)
@@ -98,14 +100,14 @@
             out[8 + r : 9 + r, :] = row[:, r * width : (r + 1) * width]
 
 
-def mod_parts(cond, cond_ctx, latent, w_shift, w_scale, w_gate):
+def mod_parts(cond, cond_ctx, latent, context, w_shift, w_scale, w_gate):
     width = w_shift.shape[1]
     shape = jax.ShapeDtypeStruct((8 + latent.shape[1] // width, width), F32)
     return call(
         mod_kernel,
-        [shape, shape],
-        [lane_rows(cond), lane_rows(cond_ctx), latent, w_shift, w_scale, w_gate],
-        [VMEM] * 6,
+        [shape, shape, jax.ShapeDtypeStruct((context.shape[0] // 2, context.shape[1]), BF16)],
+        [lane_rows(cond), lane_rows(cond_ctx), latent, context, w_shift, w_scale, w_gate],
+        [VMEM] * 7,
         flops=12 * w_shift.size,
         moved=6 * w_shift.size,
         spare=MOST,
@@ -213,11 +215,15 @@
     spent = step * jnp.exp(jnp.concatenate([decay_log[...], filler], axis=1))
     row = lax.broadcasted_iota(jnp.int32, (length, length), 0)
     col = lax.broadcasted_iota(jnp.int32, (length, length), 1)
-    lower = jnp.where(row >= col, 1.0, 0.0).astype(F32)
-    upper = jnp.where(row <= col, 1.0, 0.0).astype(F32)
-    high = lax.Precision.HIGHEST
-    prefix = jnp.dot(lower, spent, precision=high, preferred_element_type=F32)
-    suffix = jnp.dot(upper, spent, precision=high, preferred_element_type=F32)
+    lower = jnp.where(row >= col, 1.0, 0.0).astype(BF16)
+    upper = jnp.where(row <= col, 1.0, 0.0).astype(BF16)
+    prefix = suffix = 0.0
+    rest = spent
+    for _ in range(3):
+        term = rest.astype(BF16)
+        rest = rest - term.astype(F32)
+        prefix = prefix + jnp.dot(lower, term, preferred_element_type=F32)
+        suffix = suffix + jnp.dot(upper, term, preferred_element_type=F32)
     lane = lax.broadcasted_iota(jnp.int32, (length, LANES), 1)
     cum = -jnp.where(lane % 2 == 0, prefix, suffix)
     total = jnp.where(lane[0:1] % 2 == 0, cum[length - 1 : length], cum[0:1])
@@ -436,38 +442,56 @@
     )
 
 
-def project_out_kernel(count, *refs):
-    pieces, w, *rest = refs[:count], *refs[count:]
-    outs, acc = rest[:-1], rest[-1]
+def partial_out_kernel(first, *refs):
+    *pieces, w, acc = refs
     tp = lax.axis_index("tp")
     total = None
-    for q, piece in enumerate(pieces):
+    for q, piece in enumerate(pieces, first):
         depth = piece.shape[1]
-        if count > 1:
-            rows = w[pl.ds(pl.multiple_of((tp ^ q) * depth, depth), depth), :]
-        else:
-            rows = w[...]
+        rows = w[pl.ds(pl.multiple_of((tp ^ q) * depth, depth), depth), :]
         part = jnp.dot(piece[...], rows, preferred_element_type=F32)
         total = part if total is None else total + part
     acc[...] = total
+
+
+def project_out_kernel(first, *refs):
+    acc, w, *rest = refs
+    count = (len(rest) - 1 + first) // 2
+    pieces, outs, total_ref = rest[: count - first], rest[count - first : -1], rest[-1]
+    tp = lax.axis_index("tp")
+    total = acc[...]
+    for q, piece in enumerate(pieces, first):
+        depth = piece.shape[1]
+        rows = w[pl.ds(pl.multiple_of((tp ^ q) * depth, depth), depth), :]
+        total = total + jnp.dot(piece[...], rows, preferred_element_type=F32)
+    total_ref[...] = total
     block = outs[0].shape[0]
     for q, out in enumerate(outs):
-        at = pl.multiple_of((tp ^ q) * block, block) if count > 1 else 0
-        out[...] = acc[pl.ds(at, block), :].astype(BF16)
+        out[...] = total_ref[pl.ds(pl.multiple_of((tp ^ q) * block, block), block), :].astype(BF16)
 
 
 def project_out(pieces, w):
     count = len(pieces)
     length = pieces[0].shape[0]
     width = w.shape[1]
-    outs = [jax.ShapeDtypeStruct((length // count, width), BF16)] * count
+    if count == 1:
+        return [jnp.dot(pieces[0], w, preferred_element_type=F32).astype(BF16)]
+    first = count - 2
+    acc = call(
+        functools.partial(partial_out_kernel, 0),
+        jax.ShapeDtypeStruct((length, width), F32),
+        [*pieces[:first], w],
+        [VMEM] * (first + 1),
+        flops=2 * length * w.size * first // count,
+        moved=2 * w.size,
+    )
     return call(
-        functools.partial(project_out_kernel, count),
-        outs,
-        list(pieces) + [w],
-        [VMEM] * (count + 1),
+        functools.partial(project_out_kernel, first),
+        [jax.ShapeDtypeStruct((length // count, width), BF16)] * count,
+        [acc, w, *pieces[first:]],
+        [VMEM] * (2 + count - first),
         [pltpu.VMEM((length, width), F32)],
-        flops=2 * length * w.size,
+        flops=2 * length * w.size * 2 // count,
         moved=2 * w.size,
     )
 
@@ -531,7 +555,7 @@
     else:
         row_places = [((lambda sp, tp, at: at), length, None)]
 
-    up, down = mod_parts(cond, cond_ctx, latent, mod_shift_w, mod_scale_w, mod_gate_w)
+    up, down, mine = mod_parts(cond, cond_ctx, latent, context, mod_shift_w, mod_scale_w, mod_gate_w)
     received = [shift(down if k == sp_count - 1 else up, "sp", k) for k in range(1, sp_count)]
     total = up[:8]
     for part in received:
@@ -542,7 +566,6 @@
 
     if fast and ctx_own % 32 == 0:
         part = ctx_own // 2
-        mine = lax.dynamic_slice_in_dim(context, (tp & 1) * part, part, 0)
         halves = [shift(mine, "sp", k) for k in range(1, sp_count)]
     else:
         halves = None
@@ -562,7 +585,6 @@
     )
     arrived = [shift(message, "sp", k) for k, message in enumerate(messages, 1)]
     if halves is not None:
-        *halves, h = lax.optimization_barrier((*halves, h))
         ctx_pieces, ctx_places = [context], [((lambda sp, tp, at: sp * ctx_own + at), ctx_own, None)]
         for k, piece in enumerate(halves, 1):
             for bit, got in ((0, piece), (1, swap(piece, 1))):

time: 109 us -> 107 us (0.982)
  waiting for transfers between devices: 36.8 us -> 38.3 us
  starting transfers between devices: 40.9 us -> 39.5 us
  local copies, waits for them, and re-layouts: 1.22 us -> 0.09 us
    ppermute x9, starting transfers between devices: 19.5 us -> 18.2 us  [shift(): lax.ppermute(array, axis, [(i, (i + step) % count) for i in range(count)])]
    dynamic_slice x1 -> x0, local copies, waits for them, and re-layouts: 1.12 us -> none  [layer(): mine = lax.dynamic_slice_in_dim(context, (tp & 1) * part, part, 0)]
    pallas_call x8 -> x9, Pallas kernels: 27.8 us -> 27.2 us  [call(): pl.pallas_call(kernel, out_shape=outs, in_specs=specs, out_specs=jax.tree...]
  transfers between devices with their start and end apart: 40 -> 40, of which waited for: 13 -> 16; matrix products, arithmetic and copies ran while one was open for 1% -> 0% of each run, Pallas kernels for 19% -> 19%
where the time goes in v1:
time: 107 us; the launch traced here: 106 us
  starting transfers between devices  39.5 us (37%)
  waiting for transfers between devices  38.3 us (36%)
  Pallas kernels  27.2 us (25%)
    pallas_call x9, Pallas kernels, call(): pl.pallas_call(kernel, out_shape=outs, in_specs=specs, out_specs=jax.tree...  27.2 us
    ppermute x31, waiting for transfers between devices, swap(): return lax.ppermute(array, 'tp', [(i, i ^ bits) for i in range(count)])  26.6 us
    ppermute x31, starting transfers between devices, swap(): return lax.ppermute(array, 'tp', [(i, i ^ bits) for i in range(count)])  21.3 us
    ppermute x9, starting transfers between devices, shift(): lax.ppermute(array, axis, [(i, (i + step) % count) for i in range(count)])  18.2 us
    ppermute x9, waiting for transfers between devices, shift(): lax.ppermute(array, axis, [(i, (i + step) % count) for i in range(count)])  11.7 us
  transfers between devices with their start and end apart: 40, of which 16 were waited for; matrix products, arithmetic and copies ran while one was open for 0% of the time, Pallas kernels for 19%

profile of v1, /device:TPU:0, one launch (start us, length us, event | category | flops | bytes accessed | tf_op | source)
XLA Modules:
  0.0 106.1 jit_solution(8559190264092240021)
XLA Ops:
  0.0 3.4 %shard_map.190 = (f32[16,512]{1,0:T(8,128)}, f32[16,512]{1,0:T(8,128)}, bf16[32,4096]{1,0:T(8,128)(2,1)}) custom-call(bf16[8,128]{1,0:T(8,128)(2,1)} %bitcast.15, bf16[8,128]{1,0:T(8,128)(2,1)} %bitcast.16, bf16[32,4096]{1,0:T(8,128)(2,1)} %refs_8_.3, bf16[64,4096]{1,0:T(8,128)(2,1)} %refs_0_.3, bf16[1024,512]{1,0:T(8,128)(2,1)} %w_shift.1, ...), custom_call_target="tpu_custom_call" | custom-call | flops 6291456 | bytes 3145728 | tf_op jit(solution)/shard_map/pallas_call | solution.py:38
  3.4 3.1 %collective-permute-start.7 = (f32[16,512]{1,0:T(8,128)}, f32[16,512]{1,0:T(8,128)S(1)}, u32[]{:S(2)}, u32[]{:S(2)}) collective-permute-start(f32[16,512]{1,0:T(8,128)} %get-tuple-element.32), channel_id=1, source_target_pairs={{0,8},{8,16},{16,24},{24,0},{1,9},{9,17},{17,25},{25,1},{2,10},{10... | collective-permute-start | bytes 98312 | tf_op jit(solution)/shard_map/ppermute | solution.py:51
  6.4 2.6 %collective-permute-start.8 = (f32[16,512]{1,0:T(8,128)}, f32[16,512]{1,0:T(8,128)S(1)}, u32[]{:S(2)}, u32[]{:S(2)}) collective-permute-start(f32[16,512]{1,0:T(8,128)} %get-tuple-element.32), channel_id=1, source_target_pairs={{0,16},{8,24},{16,0},{24,8},{1,17},{9,25},{17,1},{25,9},{2,18},{10... | collective-permute-start | bytes 98312 | tf_op jit(solution)/shard_map/ppermute | solution.py:51
  9.0 1.3 %collective-permute-start.9 = (f32[16,512]{1,0:T(8,128)}, f32[16,512]{1,0:T(8,128)S(1)}, u32[]{:S(2)}, u32[]{:S(2)}) collective-permute-start(f32[16,512]{1,0:T(8,128)} %get-tuple-element.33), channel_id=1, source_target_pairs={{0,24},{8,0},{16,8},{24,16},{1,25},{9,1},{17,9},{25,17},{2,26},{10... | collective-permute-start | bytes 98312 | tf_op jit(solution)/shard_map/ppermute | solution.py:51
  10.6 1.2 %collective-permute-done.8 = f32[16,512]{1,0:T(8,128)S(1)} collective-permute-done((f32[16,512]{1,0:T(8,128)}, f32[16,512]{1,0:T(8,128)S(1)}, u32[]{:S(2)}, u32[]{:S(2)}) %collective-permute-start.8) | collective-permute-done | bytes 32800 | tf_op jit(solution)/shard_map/ppermute | solution.py:51
  11.8 1.3 %collective-permute-done.9 = f32[16,512]{1,0:T(8,128)S(1)} collective-permute-done((f32[16,512]{1,0:T(8,128)}, f32[16,512]{1,0:T(8,128)S(1)}, u32[]{:S(2)}, u32[]{:S(2)}) %collective-permute-start.9) | collective-permute-done | bytes 32800 | tf_op jit(solution)/shard_map/ppermute | solution.py:51
  14.0 1.6 %collective-permute-start.11 = (f32[16,512]{1,0:T(8,128)S(1)}, f32[16,512]{1,0:T(8,128)S(1)}, u32[]{:S(2)}, u32[]{:S(2)}) collective-permute-start(f32[16,512]{1,0:T(8,128)S(1)} %pad_maximum_fusion.refs_0_), channel_id=1, source_target_pairs={{0,2},{1,3},{2,0},{3,1},{4,6},{5,7},{6,4},{7,5},{8,10},{9,11},{10,... | collective-permute-start | bytes 98312 | tf_op jit(solution)/shard_map/ppermute | solution.py:56
  15.8 1.5 %collective-permute-start.13 = (f32[16,512]{1,0:T(8,128)S(1)}, f32[16,512]{1,0:T(8,128)S(1)}, u32[]{:S(2)}, u32[]{:S(2)}) collective-permute-start(f32[16,512]{1,0:T(8,128)S(1)} %pad_maximum_fusion.refs_0_), channel_id=1, source_target_pairs={{0,4},{1,5},{2,6},{3,7},{4,0},{5,1},{6,2},{7,3},{8,12},{9,13},{10,... | collective-permute-start | bytes 98312 | tf_op jit(solution)/shard_map/ppermute | solution.py:56
  17.5 2.4 %collective-permute-start.15 = (f32[16,512]{1,0:T(8,128)S(1)}, f32[16,512]{1,0:T(8,128)S(1)}, u32[]{:S(2)}, u32[]{:S(2)}) collective-permute-start(f32[16,512]{1,0:T(8,128)S(1)} %pad_maximum_fusion.refs_0_), channel_id=1, source_target_pairs={{0,6},{1,7},{2,4},{3,5},{4,2},{5,3},{6,0},{7,1},{8,14},{9,15},{10,... | collective-permute-start | bytes 98312 | tf_op jit(solution)/shard_map/ppermute | solution.py:56
  20.2 1.5 %collective-permute-start.1 = (bf16[32,4096]{1,0:T(8,128)(2,1)}, bf16[32,4096]{1,0:T(8,128)(2,1)S(1)}, u32[]{:S(2)}, u32[]{:S(2)}) collective-permute-start(bf16[32,4096]{1,0:T(8,128)(2,1)} %refs_8_.3), channel_id=1, source_target_pairs={{0,2},{1,3},{2,0},{3,1},{4,6},{5,7},{6,4},{7,5},{8,10},{9,11},{10,... | collective-permute-start | bytes 786440 | tf_op jit(solution)/shard_map/ppermute | solution.py:56
  21.7 1.5 %collective-permute-start.3 = (bf16[32,4096]{1,0:T(8,128)(2,1)}, bf16[32,4096]{1,0:T(8,128)(2,1)S(1)}, u32[]{:S(2)}, u32[]{:S(2)}) collective-permute-start(bf16[32,4096]{1,0:T(8,128)(2,1)} %refs_8_.3), channel_id=1, source_target_pairs={{0,4},{1,5},{2,6},{3,7},{4,0},{5,1},{6,2},{7,3},{8,12},{9,13},{10,... | collective-permute-start | bytes 786440 | tf_op jit(solution)/shard_map/ppermute | solution.py:56
  24.6 5.0 %collective-permute-done.1.refs_2_ = bf16[32,4096]{1,0:T(8,128)(2,1)S(1)} collective-permute-done((bf16[32,4096]{1,0:T(8,128)(2,1)}, bf16[32,4096]{1,0:T(8,128)(2,1)S(1)}, u32[]{:S(2)}, u32[]{:S(2)}) %collective-permute-start.1) | collective-permute-done | bytes 262176 | tf_op jit(solution)/shard_map/ppermute | solution.py:56
  30.5 5.4 %collective-permute-done.3.refs_4_ = bf16[32,4096]{1,0:T(8,128)(2,1)S(1)} collective-permute-done((bf16[32,4096]{1,0:T(8,128)(2,1)}, bf16[32,4096]{1,0:T(8,128)(2,1)S(1)}, u32[]{:S(2)}, u32[]{:S(2)}) %collective-permute-start.3) | collective-permute-done | bytes 262176 | tf_op jit(solution)/shard_map/ppermute | solution.py:56
  35.9 3.1 %collective-permute-start.24 = (bf16[32,4096]{1,0:T(8,128)(2,1)}, bf16[32,4096]{1,0:T(8,128)(2,1)S(1)}, u32[]{:S(2)}, u32[]{:S(2)}) collective-permute-start(bf16[32,4096]{1,0:T(8,128)(2,1)} %get-tuple-element.39), channel_id=1, source_target_pairs={{0,24},{8,0},{16,8},{24,16},{1,25},{9,1},{17,9},{25,17},{2,26},{10... | collective-permute-start | bytes 786440 | tf_op jit(solution)/shard_map/ppermute | solution.py:51
  39.8 6.6 %collective-permute-done.22.refs_3_ = bf16[32,4096]{1,0:T(8,128)(2,1)S(1)} collective-permute-done((bf16[32,4096]{1,0:T(8,128)(2,1)}, bf16[32,4096]{1,0:T(8,128)(2,1)S(1)}, u32[]{:S(2)}, u32[]{:S(2)}) %collective-permute-start.22) | collective-permute-done | bytes 262176 | tf_op jit(solution)/shard_map/ppermute | solution.py:51
  46.3 1.7 %collective-permute-done.24.refs_5_ = bf16[32,4096]{1,0:T(8,128)(2,1)S(1)} collective-permute-done((bf16[32,4096]{1,0:T(8,128)(2,1)}, bf16[32,4096]{1,0:T(8,128)(2,1)S(1)}, u32[]{:S(2)}, u32[]{:S(2)}) %collective-permute-start.24) | collective-permute-done | bytes 262176 | tf_op jit(solution)/shard_map/ppermute | solution.py:51
  48.7 7.2 %shard_map.192 = (bf16[272,4096]{1,0:T(8,128)(2,1)S(1)}, bf16[256,512]{1,0:T(8,128)(2,1)S(1)}, bf16[256,1024]{1,0:T(8,128)(2,1)S(1)}, f32[256,128]{1,0:T(8,128)S...) custom-call(bf16[32,4096]{1,0:T(8,128)(2,1)S(1)} %copy-done.5, ...), custom_call_target="tpu_custom_call" | custom-call | flops 3422552064 | bytes 12582912 | tf_op jit(solution)/shard_map/pallas_call | solution.py:38
  56.0 5.2 %shard_map.193 = (bf16[256,1024]{1,0:T(8,128)(2,1)S(1)}, f32[256,512]{1,0:T(8,128)S(1)}, f32[256,512]{1,0:T(8,128)S(1)}) custom-call(bf16[272,4096]{1,0:T(8,128)(2,1)S(1)} %get-tuple-element.40.refs_0_, bf16[256,512]{1,0:T(8,128)(2,1)S(1)} %get-tuple-element.41.refs_1_, bf16[256,1024]{1,0:T(8,128)(2,1)S(1)} %get-tuple-element.42.refs_2_, ...), custom_call_target="tpu_custom_call" | custom-call | flops 3422552064 | bytes 12582912 | tf_op jit(solution)/shard_map/pallas_call | solution.py:38
  61.2 4.5 %collective-permute-start.17 = (bf16[544,128]{1,0:T(8,128)(2,1)S(1)}, bf16[544,128]{1,0:T(8,128)(2,1)S(1)}, u32[]{:S(2)}, u32[]{:S(2)}) collective-permute-start(bf16[544,128]{1,0:T(8,128)(2,1)S(1)} %get-tuple-element.36), channel_id=1, source_target_pairs={{0,8},{8,16},{16,24},{24,0},{1,9},{9,17},{17,25},{25,1},{2,10},{10... | collective-permute-start | bytes 417800 | tf_op jit(solution)/shard_map/ppermute | solution.py:51
  65.9 2.1 %collective-permute-start.19 = (bf16[544,128]{1,0:T(8,128)(2,1)S(1)}, bf16[544,128]{1,0:T(8,128)(2,1)S(1)}, u32[]{:S(2)}, u32[]{:S(2)}) collective-permute-start(bf16[544,128]{1,0:T(8,128)(2,1)S(1)} %get-tuple-element.38), channel_id=1, source_target_pairs={{0,24},{8,0},{16,8},{24,16},{1,25},{9,1},{17,9},{25,17},{2,26},{10... | collective-permute-start | bytes 417800 | tf_op jit(solution)/shard_map/ppermute | solution.py:51
  68.1 7.0 %shard_map.194.refs_3_ = f32[1024,128]{1,0:T(8,128)S(1)} custom-call(bf16[64,4096]{1,0:T(8,128)(2,1)S(1)} %copy-done.6, bf16[32,4096]{1,0:T(8,128)(2,1)S(1)} %collective-permute-done.20.refs_1_, bf16[32,4096]{1,0:T(8,128)(2,1)S(1)} %collective-permute-done.21.refs_2_, bf16[32,4096]{1,0:T(8,128)(2,1)S(1)} %collective-permute-done.22.refs_3_, ...), custom_call_target="tpu_custom_call" | custom-call | flops 3221225472 | bytes 12582912 | tf_op jit(solution)/shard_map/pallas_call | solution.py:38
  75.7 2.2 %shard_map.195.refs_0_ = bf16[256,512]{1,0:T(8,128)(2,1)S(1)} custom-call(bf16[544,128]{1,0:T(8,128)(2,1)S(1)} %collective-permute-done.17.refs_0_, bf16[544,128]{1,0:T(8,128)(2,1)S(1)} %collective-permute-done.18.refs_1_, bf16[544,128]{1,0:T(8,128)(2,1)S(1)} %collective-permute-done.19.refs_2_, f32[1024,128]{1,0:T(8,128)S(1)} %shard_map.194.refs_3_, ...), custom_call_target="tpu_custom_call" | custom-call | flops 134217728 | bytes 1048576 | tf_op jit(solution)/shard_map/pallas_call | solution.py:38
  77.9 1.2 %collective-permute-start.27 = (bf16[256,512]{1,0:T(8,128)(2,1)S(1)}, bf16[256,512]{1,0:T(8,128)(2,1)S(1)}, u32[]{:S(2)}, u32[]{:S(2)}) collective-permute-start(bf16[256,512]{1,0:T(8,128)(2,1)S(1)} %shard_map.195.refs_0_), channel_id=1, source_target_pairs={{0,2},{1,3},{2,0},{3,1},{4,6},{5,7},{6,4},{7,5},{8,10},{9,11},{10,... | collective-permute-start | bytes 786440 | tf_op jit(solution)/shard_map/ppermute | solution.py:56
  79.1 1.5 %collective-permute-start.29 = (bf16[256,512]{1,0:T(8,128)(2,1)S(1)}, bf16[256,512]{1,0:T(8,128)(2,1)S(1)}, u32[]{:S(2)}, u32[]{:S(2)}) collective-permute-start(bf16[256,512]{1,0:T(8,128)(2,1)S(1)} %shard_map.195.refs_0_), channel_id=1, source_target_pairs={{0,4},{1,5},{2,6},{3,7},{4,0},{5,1},{6,2},{7,3},{8,12},{9,13},{10,... | collective-permute-start | bytes 786440 | tf_op jit(solution)/shard_map/ppermute | solution.py:56
  81.4 5.7 %collective-permute-done.27.refs_2_ = bf16[256,512]{1,0:T(8,128)(2,1)S(1)} collective-permute-done((bf16[256,512]{1,0:T(8,128)(2,1)S(1)}, bf16[256,512]{1,0:T(8,128)(2,1)S(1)}, u32[]{:S(2)}, u32[]{:S(2)}) %collective-permute-start.27) | collective-permute-done | bytes 262176 | tf_op jit(solution)/shard_map/ppermute | solution.py:56
  87.1 4.4 %collective-permute-done.29.refs_4_ = bf16[256,512]{1,0:T(8,128)(2,1)S(1)} collective-permute-done((bf16[256,512]{1,0:T(8,128)(2,1)S(1)}, bf16[256,512]{1,0:T(8,128)(2,1)S(1)}, u32[]{:S(2)}, u32[]{:S(2)}) %collective-permute-start.29) | collective-permute-done | bytes 262176 | tf_op jit(solution)/shard_map/ppermute | solution.py:56
  91.6 1.0 collective-permute-done.31.refs_2_
  94.8 1.2 %collective-permute-start.34 = (bf16[32,512]{1,0:T(8,128)(2,1)S(1)}, bf16[32,512]{1,0:T(8,128)(2,1)S(1)}, u32[]{:S(2)}, u32[]{:S(2)}) collective-permute-start(bf16[32,512]{1,0:T(8,128)(2,1)S(1)} %get-tuple-element.53), channel_id=1, source_target_pairs={{0,2},{1,3},{2,0},{3,1},{4,6},{5,7},{6,4},{7,5},{8,10},{9,11},{10,... | collective-permute-start | bytes 98312 | tf_op jit(solution)/shard_map/ppermute | solution.py:56
  96.5 2.5 %collective-permute-start.36 = (bf16[32,512]{1,0:T(8,128)(2,1)S(1)}, bf16[32,512]{1,0:T(8,128)(2,1)S(1)}, u32[]{:S(2)}, u32[]{:S(2)}) collective-permute-start(bf16[32,512]{1,0:T(8,128)(2,1)S(1)} %get-tuple-element.55), channel_id=1, source_target_pairs={{0,4},{1,5},{2,6},{3,7},{4,0},{5,1},{6,2},{7,3},{8,12},{9,13},{10,... | collective-permute-start | bytes 98312 | tf_op jit(solution)/shard_map/ppermute | solution.py:56
  99.0 2.0 %collective-permute-start.38 = (bf16[32,512]{1,0:T(8,128)(2,1)S(1)}, bf16[32,512]{1,0:T(8,128)(2,1)S(1)}, u32[]{:S(2)}, u32[]{:S(2)}) collective-permute-start(bf16[32,512]{1,0:T(8,128)(2,1)S(1)} %get-tuple-element.57), channel_id=1, source_target_pairs={{0,6},{1,7},{2,4},{3,5},{4,2},{5,3},{6,0},{7,1},{8,14},{9,15},{10,... | collective-permute-start | bytes 98312 | tf_op jit(solution)/shard_map/ppermute | solution.py:56
  102.4 1.5 %collective-permute-done.38.refs_6_ = bf16[32,512]{1,0:T(8,128)(2,1)S(1)} collective-permute-done((bf16[32,512]{1,0:T(8,128)(2,1)S(1)}, bf16[32,512]{1,0:T(8,128)(2,1)S(1)}, u32[]{:S(2)}, u32[]{:S(2)}) %collective-permute-start.38) | collective-permute-done | bytes 32800 | tf_op jit(solution)/shard_map/ppermute | solution.py:56
  103.8 1.5 %collective-permute-done.39.refs_7_ = bf16[32,512]{1,0:T(8,128)(2,1)S(1)} collective-permute-done((bf16[32,512]{1,0:T(8,128)(2,1)S(1)}, bf16[32,512]{1,0:T(8,128)(2,1)S(1)}, u32[]{:S(2)}, u32[]{:S(2)}) %collective-permute-start.39) | collective-permute-done | bytes 32800 | tf_op jit(solution)/shard_map/ppermute | solution.py:56
  (92 shorter events, 11.9 us)
Async XLA Ops:
  3.4 7.2 %collective-permute-start.7 = (f32[16,512]{1,0:T(8,128)}, f32[16,512]{1,0:T(8,128)S(1)}, u32[]{:S(2)}, u32[]{:S(2)}) collective-permute-start(f32[16,512]{1,0:T(8,128)} %get-tuple-element.32), channel_id=1, source_target_pairs={{0,8},{8,16},{16,24},{24,0},{1,9},{9,17},{17,25},{25,1},{2,10},{10... | collective-permute-start | bytes 98312 | tf_op jit(solution)/shard_map/ppermute | solution.py:51
  6.4 5.4 %collective-permute-start.8 = (f32[16,512]{1,0:T(8,128)}, f32[16,512]{1,0:T(8,128)S(1)}, u32[]{:S(2)}, u32[]{:S(2)}) collective-permute-start(f32[16,512]{1,0:T(8,128)} %get-tuple-element.32), channel_id=1, source_target_pairs={{0,16},{8,24},{16,0},{24,8},{1,17},{9,25},{17,1},{25,9},{2,18},{10... | collective-permute-start | bytes 98312 | tf_op jit(solution)/shard_map/ppermute | solution.py:51
  14.0 6.0 %collective-permute-start.11 = (f32[16,512]{1,0:T(8,128)S(1)}, f32[16,512]{1,0:T(8,128)S(1)}, u32[]{:S(2)}, u32[]{:S(2)}) collective-permute-start(f32[16,512]{1,0:T(8,128)S(1)} %pad_maximum_fusion.refs_0_), channel_id=1, source_target_pairs={{0,2},{1,3},{2,0},{3,1},{4,6},{5,7},{6,4},{7,5},{8,10},{9,11},{10,... | collective-permute-start | bytes 98312 | tf_op jit(solution)/shard_map/ppermute | solution.py:56
  15.5 4.7 %collective-permute-start.12 = (f32[16,512]{1,0:T(8,128)S(1)}, f32[16,512]{1,0:T(8,128)S(1)}, u32[]{:S(2)}, u32[]{:S(2)}) collective-permute-start(f32[16,512]{1,0:T(8,128)S(1)} %pad_maximum_fusion.refs_0_), channel_id=1, source_target_pairs={{0,3},{1,2},{2,1},{3,0},{4,7},{5,6},{6,5},{7,4},{8,11},{9,10},{10,... | collective-permute-start | bytes 98312 | tf_op jit(solution)/shard_map/ppermute | solution.py:56
  15.8 5.9 %collective-permute-start.13 = (f32[16,512]{1,0:T(8,128)S(1)}, f32[16,512]{1,0:T(8,128)S(1)}, u32[]{:S(2)}, u32[]{:S(2)}) collective-permute-start(f32[16,512]{1,0:T(8,128)S(1)} %pad_maximum_fusion.refs_0_), channel_id=1, source_target_pairs={{0,4},{1,5},{2,6},{3,7},{4,0},{5,1},{6,2},{7,3},{8,12},{9,13},{10,... | collective-permute-start | bytes 98312 | tf_op jit(solution)/shard_map/ppermute | solution.py:56
  17.3 5.9 %collective-permute-start.14 = (f32[16,512]{1,0:T(8,128)S(1)}, f32[16,512]{1,0:T(8,128)S(1)}, u32[]{:S(2)}, u32[]{:S(2)}) collective-permute-start(f32[16,512]{1,0:T(8,128)S(1)} %pad_maximum_fusion.refs_0_), channel_id=1, source_target_pairs={{0,5},{1,4},{2,7},{3,6},{4,1},{5,0},{6,3},{7,2},{8,13},{9,12},{10,... | collective-permute-start | bytes 98312 | tf_op jit(solution)/shard_map/ppermute | solution.py:56
  17.5 6.2 %collective-permute-start.15 = (f32[16,512]{1,0:T(8,128)S(1)}, f32[16,512]{1,0:T(8,128)S(1)}, u32[]{:S(2)}, u32[]{:S(2)}) collective-permute-start(f32[16,512]{1,0:T(8,128)S(1)} %pad_maximum_fusion.refs_0_), channel_id=1, source_target_pairs={{0,6},{1,7},{2,4},{3,5},{4,2},{5,3},{6,0},{7,1},{8,14},{9,15},{10,... | collective-permute-start | bytes 98312 | tf_op jit(solution)/shard_map/ppermute | solution.py:56
  20.2 9.4 %collective-permute-start.1 = (bf16[32,4096]{1,0:T(8,128)(2,1)}, bf16[32,4096]{1,0:T(8,128)(2,1)S(1)}, u32[]{:S(2)}, u32[]{:S(2)}) collective-permute-start(bf16[32,4096]{1,0:T(8,128)(2,1)} %refs_8_.3), channel_id=1, source_target_pairs={{0,2},{1,3},{2,0},{3,1},{4,6},{5,7},{6,4},{7,5},{8,10},{9,11},{10,... | collective-permute-start | bytes 786440 | tf_op jit(solution)/shard_map/ppermute | solution.py:56
  21.7 14.2 %collective-permute-start.3 = (bf16[32,4096]{1,0:T(8,128)(2,1)}, bf16[32,4096]{1,0:T(8,128)(2,1)S(1)}, u32[]{:S(2)}, u32[]{:S(2)}) collective-permute-start(bf16[32,4096]{1,0:T(8,128)(2,1)} %refs_8_.3), channel_id=1, source_target_pairs={{0,4},{1,5},{2,6},{3,7},{4,0},{5,1},{6,2},{7,3},{8,12},{9,13},{10,... | collective-permute-start | bytes 786440 | tf_op jit(solution)/shard_map/ppermute | solution.py:56
  23.2 15.8 %collective-permute-start.5 = (bf16[32,4096]{1,0:T(8,128)(2,1)}, bf16[32,4096]{1,0:T(8,128)(2,1)S(1)}, u32[]{:S(2)}, u32[]{:S(2)}) collective-permute-start(bf16[32,4096]{1,0:T(8,128)(2,1)} %refs_8_.3), channel_id=1, source_target_pairs={{0,6},{1,7},{2,4},{3,5},{4,2},{5,3},{6,0},{7,1},{8,14},{9,15},{10,... | collective-permute-start | bytes 786440 | tf_op jit(solution)/shard_map/ppermute | solution.py:56
  23.7 15.4 %collective-permute-start = (bf16[32,4096]{1,0:T(8,128)(2,1)}, bf16[32,4096]{1,0:T(8,128)(2,1)S(1)}, u32[]{:S(2)}, u32[]{:S(2)}) collective-permute-start(bf16[32,4096]{1,0:T(8,128)(2,1)} %refs_8_.3), channel_id=1, source_target_pairs={{0,1},{1,0},{2,3},{3,2},{4,5},{5,4},{6,7},{7,6},{8,9},{9,8},{10,11... | collective-permute-start | bytes 786440 | tf_op jit(solution)/shard_map/ppermute | solution.py:56
  24.3 15.3 %collective-permute-start.20 = (bf16[32,4096]{1,0:T(8,128)(2,1)}, bf16[32,4096]{1,0:T(8,128)(2,1)S(1)}, u32[]{:S(2)}, u32[]{:S(2)}) collective-permute-start(bf16[32,4096]{1,0:T(8,128)(2,1)} %get-tuple-element.39), channel_id=1, source_target_pairs={{0,8},{8,16},{16,24},{24,0},{1,9},{9,17},{17,25},{25,1},{2,10},{10... | collective-permute-start | bytes 786440 | tf_op jit(solution)/shard_map/ppermute | solution.py:51
  29.6 16.7 %collective-permute-start.22 = (bf16[32,4096]{1,0:T(8,128)(2,1)}, bf16[32,4096]{1,0:T(8,128)(2,1)S(1)}, u32[]{:S(2)}, u32[]{:S(2)}) collective-permute-start(bf16[32,4096]{1,0:T(8,128)(2,1)} %get-tuple-element.39), channel_id=1, source_target_pairs={{0,16},{8,24},{16,0},{24,8},{1,17},{9,25},{17,1},{25,9},{2,18},{10... | collective-permute-start | bytes 786440 | tf_op jit(solution)/shard_map/ppermute | solution.py:51
  35.9 12.1 %collective-permute-start.24 = (bf16[32,4096]{1,0:T(8,128)(2,1)}, bf16[32,4096]{1,0:T(8,128)(2,1)S(1)}, u32[]{:S(2)}, u32[]{:S(2)}) collective-permute-start(bf16[32,4096]{1,0:T(8,128)(2,1)} %get-tuple-element.39), channel_id=1, source_target_pairs={{0,24},{8,0},{16,8},{24,16},{1,25},{9,1},{17,9},{25,17},{2,26},{10... | collective-permute-start | bytes 786440 | tf_op jit(solution)/shard_map/ppermute | solution.py:51
  39.1 9.0 %collective-permute-start.2 = (bf16[32,4096]{1,0:T(8,128)(2,1)S(1)}, bf16[32,4096]{1,0:T(8,128)(2,1)S(1)}, u32[]{:S(2)}, u32[]{:S(2)}) collective-permute-start(bf16[32,4096]{1,0:T(8,128)(2,1)S(1)} %collective-permute-done.1.refs_2_), channel_id=1, source_target_pairs={{0,1},{1,0},{2,3},{3,2},{4,5},{5,4},{6,7},{7,6},{8,9},{9,8},{10,11... | collective-permute-start | bytes 786440 | tf_op jit(solution)/shard_map/ppermute | solution.py:56
  39.1 9.5 %collective-permute-start.4 = (bf16[32,4096]{1,0:T(8,128)(2,1)S(1)}, bf16[32,4096]{1,0:T(8,128)(2,1)S(1)}, u32[]{:S(2)}, u32[]{:S(2)}) collective-permute-start(bf16[32,4096]{1,0:T(8,128)(2,1)S(1)} %collective-permute-done.3.refs_4_), channel_id=1, source_target_pairs={{0,1},{1,0},{2,3},{3,2},{4,5},{5,4},{6,7},{7,6},{8,9},{9,8},{10,11... | collective-permute-start | bytes 786440 | tf_op jit(solution)/shard_map/ppermute | solution.py:56
  39.6 9.0 %collective-permute-start.6 = (bf16[32,4096]{1,0:T(8,128)(2,1)S(1)}, bf16[32,4096]{1,0:T(8,128)(2,1)S(1)}, u32[]{:S(2)}, u32[]{:S(2)}) collective-permute-start(bf16[32,4096]{1,0:T(8,128)(2,1)S(1)} %collective-permute-done.5.refs_6_), channel_id=1, source_target_pairs={{0,1},{1,0},{2,3},{3,2},{4,5},{5,4},{6,7},{7,6},{8,9},{9,8},{10,11... | collective-permute-start | bytes 786440 | tf_op jit(solution)/shard_map/ppermute | solution.py:56
  46.3 19.6 %collective-permute-start.21 = (bf16[32,4096]{1,0:T(8,128)(2,1)S(1)}, bf16[32,4096]{1,0:T(8,128)(2,1)S(1)}, u32[]{:S(2)}, u32[]{:S(2)}) collective-permute-start(bf16[32,4096]{1,0:T(8,128)(2,1)S(1)} %collective-permute-done.20.refs_1_), channel_id=1, source_target_pairs={{0,1},{1,0},{2,3},{3,2},{4,5},{5,4},{6,7},{7,6},{8,9},{9,8},{10,11... | collective-permute-start | bytes 786440 | tf_op jit(solution)/shard_map/ppermute | solution.py:56
  48.0 20.0 %collective-permute-start.23 = (bf16[32,4096]{1,0:T(8,128)(2,1)S(1)}, bf16[32,4096]{1,0:T(8,128)(2,1)S(1)}, u32[]{:S(2)}, u32[]{:S(2)}) collective-permute-start(bf16[32,4096]{1,0:T(8,128)(2,1)S(1)} %collective-permute-done.22.refs_3_), channel_id=1, source_target_pairs={{0,1},{1,0},{2,3},{3,2},{4,5},{5,4},{6,7},{7,6},{8,9},{9,8},{10,11... | collective-permute-start | bytes 786440 | tf_op jit(solution)/shard_map/ppermute | solution.py:56
  48.0 20.0 %collective-permute-start.25 = (bf16[32,4096]{1,0:T(8,128)(2,1)S(1)}, bf16[32,4096]{1,0:T(8,128)(2,1)S(1)}, u32[]{:S(2)}, u32[]{:S(2)}) collective-permute-start(bf16[32,4096]{1,0:T(8,128)(2,1)S(1)} %collective-permute-done.24.refs_5_), channel_id=1, source_target_pairs={{0,1},{1,0},{2,3},{3,2},{4,5},{5,4},{6,7},{7,6},{8,9},{9,8},{10,11... | collective-permute-start | bytes 786440 | tf_op jit(solution)/shard_map/ppermute | solution.py:56
  61.2 13.9 %collective-permute-start.17 = (bf16[544,128]{1,0:T(8,128)(2,1)S(1)}, bf16[544,128]{1,0:T(8,128)(2,1)S(1)}, u32[]{:S(2)}, u32[]{:S(2)}) collective-permute-start(bf16[544,128]{1,0:T(8,128)(2,1)S(1)} %get-tuple-element.36), channel_id=1, source_target_pairs={{0,8},{8,16},{16,24},{24,0},{1,9},{9,17},{17,25},{25,1},{2,10},{10... | collective-permute-start | bytes 417800 | tf_op jit(solution)/shard_map/ppermute | solution.py:51
  65.6 10.1 %collective-permute-start.18 = (bf16[544,128]{1,0:T(8,128)(2,1)S(1)}, bf16[544,128]{1,0:T(8,128)(2,1)S(1)}, u32[]{:S(2)}, u32[]{:S(2)}) collective-permute-start(bf16[544,128]{1,0:T(8,128)(2,1)S(1)} %get-tuple-element.37), channel_id=1, source_target_pairs={{0,16},{8,24},{16,0},{24,8},{1,17},{9,25},{17,1},{25,9},{2,18},{10... | collective-permute-start | bytes 417800 | tf_op jit(solution)/shard_map/ppermute | solution.py:51
  65.9 9.8 %collective-permute-start.19 = (bf16[544,128]{1,0:T(8,128)(2,1)S(1)}, bf16[544,128]{1,0:T(8,128)(2,1)S(1)}, u32[]{:S(2)}, u32[]{:S(2)}) collective-permute-start(bf16[544,128]{1,0:T(8,128)(2,1)S(1)} %get-tuple-element.38), channel_id=1, source_target_pairs={{0,24},{8,0},{16,8},{24,16},{1,25},{9,1},{17,9},{25,17},{2,26},{10... | collective-permute-start | bytes 417800 | tf_op jit(solution)/shard_map/ppermute | solution.py:51
  77.9 9.2 %collective-permute-start.27 = (bf16[256,512]{1,0:T(8,128)(2,1)S(1)}, bf16[256,512]{1,0:T(8,128)(2,1)S(1)}, u32[]{:S(2)}, u32[]{:S(2)}) collective-permute-start(bf16[256,512]{1,0:T(8,128)(2,1)S(1)} %shard_map.195.refs_0_), channel_id=1, source_target_pairs={{0,2},{1,3},{2,0},{3,1},{4,6},{5,7},{6,4},{7,5},{8,10},{9,11},{10,... | collective-permute-start | bytes 786440 | tf_op jit(solution)/shard_map/ppermute | solution.py:56
  79.1 12.5 %collective-permute-start.29 = (bf16[256,512]{1,0:T(8,128)(2,1)S(1)}, bf16[256,512]{1,0:T(8,128)(2,1)S(1)}, u32[]{:S(2)}, u32[]{:S(2)}) collective-permute-start(bf16[256,512]{1,0:T(8,128)(2,1)S(1)} %shard_map.195.refs_0_), channel_id=1, source_target_pairs={{0,4},{1,5},{2,6},{3,7},{4,0},{5,1},{6,2},{7,3},{8,12},{9,13},{10,... | collective-permute-start | bytes 786440 | tf_op jit(solution)/shard_map/ppermute | solution.py:56
  80.6 12.0 %collective-permute-start.31 = (bf16[256,512]{1,0:T(8,128)(2,1)S(1)}, bf16[256,512]{1,0:T(8,128)(2,1)S(1)}, u32[]{:S(2)}, u32[]{:S(2)}) collective-permute-start(bf16[256,512]{1,0:T(8,128)(2,1)S(1)} %shard_map.195.refs_0_), channel_id=1, source_target_pairs={{0,6},{1,7},{2,4},{3,5},{4,2},{5,3},{6,0},{7,1},{8,14},{9,15},{10,... | collective-permute-start | bytes 786440 | tf_op jit(solution)/shard_map/ppermute | solution.py:56
  81.4 11.1 %collective-permute-start.26 = (bf16[256,512]{1,0:T(8,128)(2,1)S(1)}, bf16[256,512]{1,0:T(8,128)(2,1)S(1)}, u32[]{:S(2)}, u32[]{:S(2)}) collective-permute-start(bf16[256,512]{1,0:T(8,128)(2,1)S(1)} %shard_map.195.refs_0_), channel_id=1, source_target_pairs={{0,1},{1,0},{2,3},{3,2},{4,5},{5,4},{6,7},{7,6},{8,9},{9,8},{10,11... | collective-permute-start | bytes 786440 | tf_op jit(solution)/shard_map/ppermute | solution.py:56
  87.1 5.4 %collective-permute-start.28 = (bf16[256,512]{1,0:T(8,128)(2,1)S(1)}, bf16[256,512]{1,0:T(8,128)(2,1)S(1)}, u32[]{:S(2)}, u32[]{:S(2)}) collective-permute-start(bf16[256,512]{1,0:T(8,128)(2,1)S(1)} %collective-permute-done.27.refs_2_), channel_id=1, source_target_pairs={{0,1},{1,0},{2,3},{3,2},{4,5},{5,4},{6,7},{7,6},{8,9},{9,8},{10,11... | collective-permute-start | bytes 786440 | tf_op jit(solution)/shard_map/ppermute | solution.py:56
  94.8 6.2 %collective-permute-start.34 = (bf16[32,512]{1,0:T(8,128)(2,1)S(1)}, bf16[32,512]{1,0:T(8,128)(2,1)S(1)}, u32[]{:S(2)}, u32[]{:S(2)}) collective-permute-start(bf16[32,512]{1,0:T(8,128)(2,1)S(1)} %get-tuple-element.53), channel_id=1, source_target_pairs={{0,2},{1,3},{2,0},{3,1},{4,6},{5,7},{6,4},{7,5},{8,10},{9,11},{10,... | collective-permute-start | bytes 98312 | tf_op jit(solution)/shard_map/ppermute | solution.py:56
  96.0 5.4 %collective-permute-start.35 = (bf16[32,512]{1,0:T(8,128)(2,1)S(1)}, bf16[32,512]{1,0:T(8,128)(2,1)S(1)}, u32[]{:S(2)}, u32[]{:S(2)}) collective-permute-start(bf16[32,512]{1,0:T(8,128)(2,1)S(1)} %get-tuple-element.54), channel_id=1, source_target_pairs={{0,3},{1,2},{2,1},{3,0},{4,7},{5,6},{6,5},{7,4},{8,11},{9,10},{10,... | collective-permute-start | bytes 98312 | tf_op jit(solution)/shard_map/ppermute | solution.py:56
  96.5 4.9 %collective-permute-start.36 = (bf16[32,512]{1,0:T(8,128)(2,1)S(1)}, bf16[32,512]{1,0:T(8,128)(2,1)S(1)}, u32[]{:S(2)}, u32[]{:S(2)}) collective-permute-start(bf16[32,512]{1,0:T(8,128)(2,1)S(1)} %get-tuple-element.55), channel_id=1, source_target_pairs={{0,4},{1,5},{2,6},{3,7},{4,0},{5,1},{6,2},{7,3},{8,12},{9,13},{10,... | collective-permute-start | bytes 98312 | tf_op jit(solution)/shard_map/ppermute | solution.py:56
  99.0 4.8 %collective-permute-start.38 = (bf16[32,512]{1,0:T(8,128)(2,1)S(1)}, bf16[32,512]{1,0:T(8,128)(2,1)S(1)}, u32[]{:S(2)}, u32[]{:S(2)}) collective-permute-start(bf16[32,512]{1,0:T(8,128)(2,1)S(1)} %get-tuple-element.57), channel_id=1, source_target_pairs={{0,6},{1,7},{2,4},{3,5},{4,2},{5,3},{6,0},{7,1},{8,14},{9,15},{10,... | collective-permute-start | bytes 98312 | tf_op jit(solution)/shard_map/ppermute | solution.py:56
  (24 other events, 339.4 us)
